TPU v7x, 32 devices: a whole 2x2x4 slice. The times are simulated.
32 devices in a mesh: sp: 16 (over z, y, x), tp: 2 (over core).
Axes of the slice: x: 2, y: 2, z: 4, core: 2. Of those that a mesh axis runs over, the one named last changes fastest.
Arguments:
- normed: bfloat16 [4096, 2048], P(('sp', 'tp')), may hold values from -40 to 40
- query_weight: bfloat16 [2048, 2048], P(None, 'tp'), may hold values from -1.5 to 1.5
- key_weight: bfloat16 [2048, 2048], P(None, 'tp'), may hold values from -1 to 1
- value_weight: bfloat16 [2048, 2048], P(None, 'tp'), may hold values from -0.125 to 0.125
- pool_in_weight: bfloat16 [2048, 1024], P(None, 'tp'), may hold values from -0.125 to 0.125
- pool_weight: bfloat16 [8, 128, 128], P('tp'), may hold values from -0.5 to 0.5
- map_balance: float32 [8], replicated, may hold values from 0.3 to 0.8
- head_gain: float32 [256], replicated, may hold values from 0.1 to 1.9
- contrast_out_weight: bfloat16 [2048, 2048], P('tp'), may hold values from -0.109375 to 0.109375
- pool_out_weight: bfloat16 [1024, 2048], P('tp'), may hold values from -0.109375 to 0.109375
Outputs:
- layer_out: bfloat16 [4096, 2048], P(('sp', 'tp'))
All inputs are finite; a program needn't handle non-finite values.
Results may differ from a plain program's by a relative error of at most 0.03.
Values may be sent and summed in bfloat16 or wider, within the bound.
A program may use at most 128 MiB of HBM per device.

v0:
```python
import functools
import math

import jax
import jax.numpy as jnp
from jax import lax
from jax.experimental import pallas as pl
from jax.experimental.pallas import tpu as pltpu
from jax.sharding import PartitionSpec as P

reach_back = 15
norm_epsilon = 1e-06


def passed_along(block, axis, distance):
    devices = range(lax.axis_size(axis))
    route = [(i - distance, i) for i in devices if i - distance in devices]
    return lax.ppermute(block, axis, route)


def from_partner(block, axis, stride):
    count = lax.axis_size(axis)
    route = []
    for low in range(count):
        high = low | 1 << stride
        if high != low and high < count:
            route += [(low, high), (high, low)]
    return lax.ppermute(block, axis, route)


def shifted(array, axis, by):
    size = lax.axis_size(axis)
    return lax.ppermute(array, axis, [(i, (i + by) % size) for i in range(size)])


def as_sent(array):

    def short(part):
        return part.astype(jnp.bfloat16) if part.dtype == jnp.float32 else part

    return jax.tree.map(short, array)


def attend(running, queries, key_rows, value_rows, query_first, key_first, score_scale):
    key_count = key_rows.shape[0]
    key_block = math.gcd(key_count, 1024)
    unit_count = queries.shape[1]
    heads_here = value_rows.shape[1]
    per_head = unit_count // heads_here
    query_count = queries.shape[0]
    query_order = query_first + lax.iota(jnp.int32, query_count)

    def key_step(block_index, carried):
        block_start = block_index * key_block

        def block_work(current):
            row_peak, row_total, weighted = current
            scores = (
                jnp.einsum("qud,kud->uqk", queries, key_rows, preferred_element_type=jnp.float32)
                * score_scale
            )
            key_order = key_first + block_start + lax.iota(jnp.int32, key_block)
            scores = jnp.where(
                key_order[None, None, :] <= query_order[None, :, None], scores, -jnp.inf
            )
            new_peak = jnp.maximum(row_peak, jnp.max(scores, axis=2))
            shrink = jnp.exp(row_peak - new_peak)
            raised = jnp.exp(scores - new_peak[:, :, None])
            row_total = row_total * shrink + jnp.sum(raised, axis=2)
            map_weights = raised.astype(jnp.bfloat16).reshape(
                heads_here, per_head, query_count, key_block
            )
            update = jnp.einsum(
                "hmqk,khe->hmqe", map_weights, value_rows, preferred_element_type=jnp.float32
            )
            weighted = weighted * shrink[:, :, None] + update.reshape(unit_count, query_count, -1)
            return (new_peak, row_total, weighted)

        def keep_state(current):
            return current

        return lax.cond(
            key_first + block_start <= query_first + query_count - 1,
            block_work,
            keep_state,
            carried,
        )

    return lax.fori_loop(0, key_count // key_block, key_step, running)


def fresh_state(unit_count, row_count, value_width):
    return (
        jnp.full((unit_count, row_count), -1e30, jnp.float32),
        jnp.zeros((unit_count, row_count), jnp.float32),
        jnp.zeros((unit_count, row_count, value_width), jnp.float32),
    )


def finished(running):
    row_peak, row_total, weighted = running
    return (weighted / row_total[:, :, None]).astype(jnp.bfloat16)


def joined_state(first, second):
    first_peak, first_total, first_weighted = first
    second_peak, second_total, second_weighted = second
    new_peak = jnp.maximum(first_peak, second_peak)
    first_shrink = jnp.exp(first_peak - new_peak)
    second_shrink = jnp.exp(second_peak - new_peak)
    new_total = first_total * first_shrink + second_total * second_shrink
    new_weighted = (
        first_weighted * first_shrink[:, :, None] + second_weighted * second_shrink[:, :, None]
    )
    return (new_peak, new_total, new_weighted)


def per_device(
    normed,
    query_weight,
    key_weight,
    value_weight,
    pool_in_weight,
    pool_weight,
    map_balance,
    head_gain,
    contrast_out_weight,
    pool_out_weight,
):
    tp_index = lax.axis_index("tp")
    sp_count = lax.axis_size("sp")
    sp_index = lax.axis_index("sp")
    head_dim = head_gain.shape[0] // 2
    value_width = 2 * head_dim
    query_cols = query_weight.shape[1]
    value_cols = value_weight.shape[1]
    unit_count = query_cols // head_dim
    heads_here = unit_count // 2
    project_incoming = lax.all_gather(normed, "tp", axis=0, tiled=True)
    products = [
        jnp.dot(project_incoming, weight_part, preferred_element_type=jnp.float32)
        for weight_part in (query_weight, key_weight, value_weight, pool_in_weight)
    ]
    joined = jnp.concatenate(products, axis=1).astype(jnp.bfloat16)
    row_count = joined.shape[0]
    queries = joined[:, :query_cols].reshape(row_count, unit_count, head_dim)
    key_rows = joined[:, query_cols : 2 * query_cols].reshape(row_count, unit_count, head_dim)
    value_rows = joined[:, 2 * query_cols : 2 * query_cols + value_cols].reshape(
        row_count, heads_here, value_width
    )
    pool_input = joined[:, 2 * query_cols + value_cols :]
    pool_cols = pool_input.shape[1]
    upper_rim = passed_along(pool_input[row_count - reach_back :], "sp", 1)
    extended = jnp.concatenate([upper_rim, pool_input], axis=0).astype(jnp.float32)
    groups_here = pool_weight.shape[0]
    group_width = pool_weight.shape[1]
    group_index = tp_index * groups_here + lax.iota(jnp.int32, pool_cols) // group_width
    widths = jnp.left_shift(jnp.int32(2), group_index % 4)
    window_sum = jnp.zeros((row_count, pool_cols), jnp.float32)
    for offset in range(reach_back + 1):
        window_sum = window_sum + extended[
            reach_back - offset : reach_back - offset + row_count
        ] * (offset < widths)[None, :].astype(jnp.float32)
    position = sp_index * row_count + lax.iota(jnp.int32, row_count)
    counts = jnp.minimum(position[:, None] + 1, widths[None, :]).astype(jnp.float32)
    spread = (window_sum / counts - extended[reach_back:]).astype(jnp.bfloat16)
    mixed_groups = jnp.einsum(
        "tgc,gce->tge",
        spread.reshape(row_count, groups_here, group_width),
        pool_weight,
        preferred_element_type=jnp.float32,
    )
    pool_out = mixed_groups.reshape(row_count, pool_cols).astype(jnp.bfloat16)
    score_scale = head_dim ** (-0.5)
    level_count = sp_count.bit_length() - 1
    low_levels = level_count // 2
    band_size = 1 << low_levels
    band_count = sp_count // band_size
    member = sp_index % band_size
    band = sp_index // band_size
    band_queries = queries
    for bit in range(low_levels):
        received = from_partner(band_queries, "sp", bit)
        upper = member >> bit & 1 == 1
        band_queries = jnp.where(
            upper,
            jnp.concatenate([received, band_queries], axis=0),
            jnp.concatenate([band_queries, received], axis=0),
        )
    band_first = band * band_size * row_count
    running = fresh_state(unit_count, band_size * row_count, value_width)
    for step in range(band_count):
        if step == 0:
            key_piece, value_piece = (key_rows, value_rows)
        else:
            key_piece, value_piece = shifted((key_rows, value_rows), "sp", step * band_size)
        source = (sp_index - step * band_size) % sp_count
        running = attend(
            running,
            band_queries,
            key_piece,
            value_piece,
            band_first,
            source * row_count,
            score_scale,
        )
    for bit in range(low_levels - 1, -1, -1):
        half = running[0].shape[1] // 2
        upper = member >> bit & 1 == 1
        lower_part = jax.tree.map(lambda item: item[:, :half], running)
        upper_part = jax.tree.map(lambda item: item[:, half:], running)
        outgoing = jax.tree.map(
            lambda low, high: jnp.where(upper, low, high), lower_part, upper_part
        )
        kept = jax.tree.map(lambda low, high: jnp.where(upper, high, low), lower_part, upper_part)
        incoming = from_partner(
            (as_sent(outgoing[0]), as_sent(outgoing[1]), as_sent(outgoing[2])), "sp", bit
        )
        running = joined_state(kept, incoming)
    maps = finished(running)
    paired = maps.reshape(heads_here, 2, row_count, value_width)
    paired = lax.optimization_barrier(paired).astype(jnp.float32)
    head_first = tp_index * heads_here
    balance_here = lax.dynamic_slice_in_dim(map_balance, head_first, heads_here, 0)
    contrast = paired[:, 0] - balance_here[:, None, None] * paired[:, 1]
    mean_square = jnp.mean(contrast * contrast, axis=2, keepdims=True)
    contrast = contrast * lax.rsqrt(mean_square + norm_epsilon) * head_gain
    contrast_out = (
        contrast.astype(jnp.bfloat16)
        .transpose(1, 0, 2)
        .reshape(row_count, heads_here * value_width)
    )
    partial_value = jnp.dot(contrast_out, contrast_out_weight, preferred_element_type=jnp.float32)
    return lax.psum_scatter(
        (
            partial_value + jnp.dot(pool_out, pool_out_weight, preferred_element_type=jnp.float32)
        ).astype(jnp.bfloat16),
        "tp",
        scatter_dimension=0,
        tiled=True,
    )


MESH = pl.DeviceIdType.MESH


def flipped(index, mask, size):
    total = 0
    bit = 1
    while bit < size:
        total = total + lax.rem(lax.div(index, bit) + lax.div(mask, bit), 2) * bit
        bit *= 2
    return total


def layer_kernel(
    sp_count,
    members,
    x_ref,
    pool_weight,
    balance,
    gain,
    query_hbm,
    key_hbm,
    value_hbm,
    pool_in_hbm,
    contrast_hbm,
    pool_out_hbm,
    out_ref,
    out_recv,
    query_w,
    key_w,
    value_w,
    pool_in_w,
    contrast_w,
    pool_out_w,
    rows_in,
    kv,
    kv_stage,
    queries,
    query_stage,
    peaks,
    totals,
    weighted,
    contrasts,
    contrast_stage,
    rim,
    rim_stage,
    pool_part,
    out_stage,
    weight_sem,
    local_sem,
    pair_send,
    pair_recv,
    relay_send,
    relay_recv,
    kv_send,
    kv_recv,
    query_send,
    query_recv,
    contrast_send,
    contrast_recv,
    rim_send,
    rim_recv,
    out_send,
    out_recv_sem,
):
    f32 = jnp.float32
    bf16 = jnp.bfloat16
    bands = sp_count // members
    sp = lax.axis_index("sp")
    tp = lax.axis_index("tp")
    other = 1 - tp
    band = lax.div(sp, members)
    member = lax.rem(sp, members)
    half, model = x_ref.shape
    rows = 2 * half
    width = gain.shape[1]
    head_dim = width // 2

    loads = [
        pltpu.make_async_copy(src, dst, weight_sem.at[i])
        for i, (src, dst) in enumerate(
            (
                (key_hbm, key_w),
                (value_hbm, value_w),
                (query_hbm, query_w),
                (pool_in_hbm, pool_in_w),
                (pool_out_hbm, pool_out_w),
                (contrast_hbm, contrast_w),
            )
        )
    ]
    for load in loads:
        load.start()
    keep = pltpu.make_async_copy(x_ref, rows_in.at[0, tp], local_sem)
    keep.start()

    barrier = pltpu.get_barrier_semaphore()
    greeted = [
        (sp, other),
        (lax.rem(sp + members, sp_count), tp),
        (lax.rem(sp + sp_count - members, sp_count), tp),
        (lax.rem(sp + 1, sp_count), tp),
        (lax.rem(sp + sp_count - 1, sp_count), tp),
    ]
    greeted += [(band * members + flipped(member, j, members), tp) for j in range(1, members)]
    for target in greeted:
        pl.semaphore_signal(barrier, inc=1, device_id=target, device_id_type=MESH)
    pl.semaphore_wait(barrier, len(greeted))

    def pair_copy(step):
        return pltpu.make_async_remote_copy(
            src_ref=x_ref if step == 0 else rows_in.at[step, tp],
            dst_ref=rows_in.at[step, tp],
            send_sem=pair_send.at[step],
            recv_sem=pair_recv.at[step],
            device_id=(sp, other),
            device_id_type=MESH,
        )

    def relay_copy(step):
        return pltpu.make_async_remote_copy(
            src_ref=x_ref if step == 1 else rows_in.at[step - 1, tp],
            dst_ref=rows_in.at[step, tp],
            send_sem=relay_send.at[step],
            recv_sem=relay_recv.at[step],
            device_id=(lax.rem(sp + members, sp_count), tp),
            device_id_type=MESH,
        )

    def kv_copy(step, j):
        return pltpu.make_async_remote_copy(
            src_ref=kv_stage.at[step, j],
            dst_ref=kv.at[step, member],
            send_sem=kv_send.at[step, j],
            recv_sem=kv_recv.at[step, j],
            device_id=(band * members + flipped(member, j, members), tp),
            device_id_type=MESH,
        )

    def query_copy(j):
        return pltpu.make_async_remote_copy(
            src_ref=query_stage.at[j],
            dst_ref=queries.at[member],
            send_sem=query_send.at[j],
            recv_sem=query_recv.at[j],
            device_id=(band * members + flipped(member, j, members), tp),
            device_id_type=MESH,
        )

    def contrast_copy(j):
        return pltpu.make_async_remote_copy(
            src_ref=contrast_stage.at[j],
            dst_ref=contrasts.at[member],
            send_sem=contrast_send.at[j],
            recv_sem=contrast_recv.at[j],
            device_id=(band * members + flipped(member, j, members), tp),
            device_id_type=MESH,
        )

    rim_copy = pltpu.make_async_remote_copy(
        src_ref=rim_stage,
        dst_ref=rim,
        send_sem=rim_send,
        recv_sem=rim_recv,
        device_id=(lax.rem(sp + 1, sp_count), tp),
        device_id_type=MESH,
    )
    out_copy = pltpu.make_async_remote_copy(
        src_ref=out_stage,
        dst_ref=out_recv,
        send_sem=out_send,
        recv_sem=out_recv_sem,
        device_id=(sp, other),
        device_id_type=MESH,
    )

    pair_copy(0).start()

    @pl.when(band + 1 < bands)
    def _():
        relay_copy(1).start()

    def project(step):
        def one(t, carry):
            j = lax.rem(t + 1, members)
            head = flipped(member, j, members)
            columns = pl.ds(pl.multiple_of(head * width, width), width)
            x = rows_in[step].reshape(rows, model)
            keys = jnp.dot(x, key_w[:, columns], preferred_element_type=f32).astype(bf16)
            values = jnp.dot(x, value_w[:, columns], preferred_element_type=f32).astype(bf16)

            @pl.when(j > 0)
            def _():
                kv_stage[step, j, :, :width] = keys
                kv_stage[step, j, :, width:] = values
                kv_copy(step, j).start()

            @pl.when(j == 0)
            def _():
                kv[step, member, :, :width] = keys
                kv[step, member, :, width:] = values

            if step == 0:
                mine = jnp.dot(x, query_w[:, columns], preferred_element_type=f32).astype(bf16)

                @pl.when(j > 0)
                def _():
                    query_stage[j] = mine
                    query_copy(j).start()

                @pl.when(j == 0)
                def _():
                    queries[member] = mine

            return carry

        lax.fori_loop(0, members, one, 0)

    def take_band(step):
        @pl.when(band >= step)
        def _():
            relay_copy(step).wait_recv()
            if step + 1 < bands:

                @pl.when(band + 1 < bands)
                def _():
                    relay_copy(step + 1).start()

            pair_copy(step).start()
            pair_copy(step).wait_recv()
            project(step)

    log_scale = head_dim ** (-0.5) * math.log2(math.e)

    def attend_block(step, i, blocks):
        seen = len(blocks)
        for u in range(2):
            cols = slice(u * head_dim, (u + 1) * head_dim)
            keys = jnp.concatenate([kv[step, b, :, cols] for b in blocks], axis=0)
            values = jnp.concatenate([kv[step, b, :, width:] for b in blocks], axis=0)
            scores = lax.dot_general(
                queries[i, :, cols], keys, (((1,), (1,)), ((), ())), preferred_element_type=f32
            )
            if step == 0:
                query_order = lax.broadcasted_iota(jnp.int32, scores.shape, 0) + (seen - 1) * rows
                key_order = lax.broadcasted_iota(jnp.int32, scores.shape, 1)
                scores = jnp.where(key_order <= query_order, scores, -jnp.inf)
            peak = jnp.max(scores, axis=1, keepdims=True)
            if step > 0:
                old = peaks[u, i][:, :1]
                peak = jnp.maximum(peak, old)
                shrink = jnp.exp2((old - peak) * log_scale)
            raised = jnp.exp2((scores - peak) * log_scale)
            total = jnp.sum(raised, axis=1, keepdims=True)
            update = jnp.dot(raised.astype(bf16), values, preferred_element_type=f32)
            if step > 0:
                total = total + totals[u, i][:, :1] * shrink
                update = update + weighted[u, i] * shrink
            peaks[u, i] = jnp.broadcast_to(peak, peaks.shape[2:])
            totals[u, i] = jnp.broadcast_to(total, totals.shape[2:])
            weighted[u, i] = update

    weight = balance[tp * members + member]

    def finish(i, j):
        first = (weighted[0, i] / totals[0, i][:, :1]).astype(bf16).astype(f32)
        second = (weighted[1, i] / totals[1, i][:, :1]).astype(bf16).astype(f32)
        contrast = first - weight * second
        mean_square = jnp.mean(contrast * contrast, axis=1, keepdims=True)
        result = (contrast * lax.rsqrt(mean_square + norm_epsilon) * gain[...]).astype(bf16)

        @pl.when(j > 0)
        def _():
            contrast_stage[j] = result
            contrast_copy(j).start()

        @pl.when(j == 0)
        def _():
            contrasts[member] = result

    def attend_own():
        for j in range(1, members):
            query_copy(j).wait_recv()
            kv_copy(0, j).wait_recv()
        for i in range(members):
            attend_block(0, i, list(range(i + 1)))

            @pl.when(band == 0)
            def _(i=i):
                finish(i, flipped(member, i, members))

    parts = (list(range(members)),)

    def attend_band(step):
        @pl.when(band >= step)
        def _():
            for part in parts:
                for j in part:
                    if j > 0:
                        kv_copy(step, j).wait_recv()
                blocks = [flipped(member, j, members) for j in part]

                def one(t, carry, part=part, blocks=blocks):
                    j = lax.rem(t + 1, members)
                    i = flipped(member, j, members)
                    attend_block(step, i, blocks)
                    if part is parts[-1]:

                        @pl.when(band == step)
                        def _():
                            finish(i, j)

                    return carry

                lax.fori_loop(0, members, one, 0)

    keep.wait()
    loads[0].wait()
    loads[1].wait()
    loads[2].wait()
    pair_copy(0).wait_recv()
    project(0)

    loads[3].wait()
    pool_input = jnp.dot(
        rows_in[0].reshape(rows, model), pool_in_w[...], preferred_element_type=f32
    ).astype(bf16)
    rim_stage[...] = pool_input[rows - rim.shape[0] :]

    @pl.when(sp + 1 < sp_count)
    def _():
        rim_copy.start()

    take_band(1)

    @pl.when(sp > 0)
    def _():
        rim_copy.wait_recv()

    @pl.when(sp == 0)
    def _():
        rim[...] = jnp.zeros_like(rim)

    loads[4].wait()
    extended = jnp.concatenate([rim[...], pool_input], axis=0).astype(f32)
    group_width = pool_weight.shape[1]
    skirt = rim.shape[0]
    position = sp * rows + lax.broadcasted_iota(jnp.int32, (rows, group_width), 0)
    mixed = []
    for group in range(pool_weight.shape[0]):
        block = extended[:, group * group_width : (group + 1) * group_width]
        window = block
        reach = 1
        span = 2 ** (1 + group % 4)
        while reach < span:
            window = window + pltpu.roll(window, reach, 0)
            reach *= 2
        counts = jnp.minimum(position + 1, span).astype(f32)
        spread = (window[skirt:] / counts - block[skirt:]).astype(bf16)
        mixed.append(
            jnp.dot(spread, pool_weight[group], preferred_element_type=f32).astype(bf16)
        )
    pool_out = jnp.concatenate(mixed, axis=1)
    chunk = math.gcd(model, 512)
    for start in range(0, model, chunk):
        pool_part[:, start : start + chunk] = jnp.dot(
            pool_out, pool_out_w[:, start : start + chunk], preferred_element_type=f32
        )

    for step in range(2, bands):
        take_band(step)
        if step == 2:
            attend_own()
        else:
            attend_band(step - 2)
    if bands == 2:
        attend_own()
    for step in range(max(bands - 2, 1), bands):
        attend_band(step)

    loads[5].wait()
    for j in range(1, members):
        contrast_copy(j).wait_recv()

    def projected(side, store):
        taken = pl.ds(pl.multiple_of(side * half, half), half)
        left = jnp.concatenate([contrasts[h, taken, :] for h in range(members)], axis=1)
        for start in range(0, model, chunk):
            cut = slice(start, start + chunk)
            part = jnp.dot(left, contrast_w[:, cut], preferred_element_type=f32)
            store(cut, (part + pool_part[taken, cut]).astype(bf16))

    def to_partner(cut, part):
        out_stage[:, cut] = part

    def to_self(cut, part):
        out_ref[:, cut] = part

    projected(other, to_partner)
    out_copy.start()
    projected(tp, to_self)
    out_copy.wait()
    pair_copy(0).wait_send()
    for j in range(1, members):
        query_copy(j).wait_send()
        kv_copy(0, j).wait_send()
        contrast_copy(j).wait_send()

    @pl.when(sp + 1 < sp_count)
    def _():
        rim_copy.wait_send()

    for step in range(1, bands):

        @pl.when(jnp.logical_and(band + 1 < bands, band >= step - 1))
        def _(step=step):
            relay_copy(step).wait_send()

        @pl.when(band >= step)
        def _(step=step):
            pair_copy(step).wait_send()
            for j in range(1, members):
                kv_copy(step, j).wait_send()


def kernel_scratch(sp_count, members, half, model, width, pool_cols):
    bf16 = jnp.bfloat16
    bands = sp_count // members
    rows = 2 * half
    columns = members * width
    dma = pltpu.SemaphoreType.DMA
    return [
        pltpu.VMEM((model, columns), bf16),
        pltpu.VMEM((model, columns), bf16),
        pltpu.VMEM((model, columns), bf16),
        pltpu.VMEM((model, pool_cols), bf16),
        pltpu.VMEM((columns, model), bf16),
        pltpu.VMEM((pool_cols, model), bf16),
        pltpu.VMEM((bands, 2, half, model), bf16),
        pltpu.VMEM((bands, members, rows, 2 * width), bf16),
        pltpu.VMEM((bands, members, rows, 2 * width), bf16),
        pltpu.VMEM((members, rows, width), bf16),
        pltpu.VMEM((members, rows, width), bf16),
        pltpu.VMEM((2, members, rows, 128), jnp.float32),
        pltpu.VMEM((2, members, rows, 128), jnp.float32),
        pltpu.VMEM((2, members, rows, width), jnp.float32),
        pltpu.VMEM((members, rows, width), bf16),
        pltpu.VMEM((members, rows, width), bf16),
        pltpu.VMEM((reach_back + 1, pool_cols), bf16),
        pltpu.VMEM((reach_back + 1, pool_cols), bf16),
        pltpu.VMEM((rows, model), jnp.float32),
        pltpu.VMEM((half, model), bf16),
        dma((6,)),
        dma,
        dma((bands,)),
        dma((bands,)),
        dma((bands,)),
        dma((bands,)),
        dma((bands, members)),
        dma((bands, members)),
        dma((members,)),
        dma((members,)),
        dma((members,)),
        dma((members,)),
        dma,
        dma,
        dma,
        dma,
    ]


vmem_most = 67043328


def scratch_bytes(scratch):
    return sum(
        math.prod(item.shape) * jnp.dtype(item.dtype).itemsize
        for item in scratch
        if getattr(item, "memory_space", None) == pltpu.VMEM
    )


def whole_layer(
    normed,
    query_weight,
    key_weight,
    value_weight,
    pool_in_weight,
    pool_weight,
    map_balance,
    head_gain,
    contrast_out_weight,
    pool_out_weight,
):
    sp_count = lax.axis_size("sp")
    width = head_gain.shape[0]
    members = query_weight.shape[1] // width
    half, model = normed.shape
    pool_cols = pool_in_weight.shape[1]
    groups_here = pool_weight.shape[0]
    scratch = kernel_scratch(
        sp_count, max(members, 1), half, model, width, pool_cols
    )
    fits = (
        lax.axis_size("tp") == 2
        and members > 1
        and members & (members - 1) == 0
        and sp_count % members == 0
        and sp_count // members > 1
        and groups_here % 4 == 0
        and scratch_bytes(scratch) < vmem_most * 3 // 4
    )
    if not fits:
        return per_device(
            normed,
            query_weight,
            key_weight,
            value_weight,
            pool_in_weight,
            pool_weight,
            map_balance,
            head_gain,
            contrast_out_weight,
            pool_out_weight,
        )
    vmem = pl.BlockSpec(memory_space=pltpu.VMEM)
    hbm = pl.BlockSpec(memory_space=pl.ANY)
    own_part, partner_part = pl.pallas_call(
        functools.partial(layer_kernel, sp_count, members),
        out_shape=[jax.ShapeDtypeStruct((half, model), jnp.bfloat16)] * 2,
        in_specs=[vmem, vmem, pl.BlockSpec(memory_space=pltpu.SMEM), vmem] + [hbm] * 6,
        out_specs=[vmem, vmem],
        scratch_shapes=scratch,
        compiler_params=pltpu.CompilerParams(
            collective_id=0, has_side_effects=True, vmem_limit_bytes=vmem_most
        ),
    )(
        normed,
        pool_weight,
        map_balance,
        head_gain.reshape(1, width),
        query_weight,
        key_weight,
        value_weight,
        pool_in_weight,
        contrast_out_weight,
        pool_out_weight,
    )
    return (own_part.astype(jnp.float32) + partner_part.astype(jnp.float32)).astype(jnp.bfloat16)


def solution(mesh):
    return jax.shard_map(
        whole_layer,
        mesh=mesh,
        in_specs=(
            P(("sp", "tp"), None),
            P(None, "tp"),
            P(None, "tp"),
            P(None, "tp"),
            P(None, "tp"),
            P("tp", None, None),
            P(),
            P(),
            P("tp", None),
            P("tp", None),
        ),
        out_specs=P(("sp", "tp"), None),
        check_vma=False,
    )
```

profile of v0, /device:TPU:25, one launch (start us, length us, event | category | flops | bytes accessed | tf_op | source)
XLA Modules:
  0.0 77.7 jit_solution(8664566973585230077)
XLA Ops:
  0.0 75.6 %shard_map.100 = (bf16[128,2048]{1,0:T(8,128)(2,1)}, bf16[128,2048]{1,0:T(8,128)(2,1)}) custom-call(bf16[128,2048]{1,0:T(8,128)(2,1)} %x_ref.1, bf16[4,128,128]{2,1,0:T(8,128)(2,1)} %pool_weight.1, f32[8]{0:T(128)} %balance.1, f32[1,256]{1,0:T(1,128)} %bitcast.1, bf16[2048,1024]{1,0:T(8,128)(2,1)} %query_hbm.1, bf16[2048,1024]{1,0:T(8,128)(2,1)} %key_hbm.1, ...), custom_call_target="tpu_custom_call" | custom-call | tf_op jit(solution)/shard_map/pallas_call | solution.py:770
  75.6 2.1 %add_convert_fusion = bf16[128,2048]{1,0:T(8,128)(2,1)} fusion(bf16[128,2048]{1,0:T(8,128)(2,1)} %get-tuple-element.8, bf16[128,2048]{1,0:T(8,128)(2,1)} %get-tuple-element.7), kind=kLoop, calls=%fused_computation | loop fusion | flops 1048576 | bytes 1572864 | tf_op jit(solution)/shard_map/convert_element_type | solution.py:791
where the time goes:
time: 77.9 us; the launch traced here: 77.7 us
  Pallas kernels  75.6 us (97%)
  other arithmetic  2.12 us (3%)
    pallas_call x1, Pallas kernels, whole_layer(): pl.pallas_call(functools.partial(layer_kernel, sp_count, members), out_sh...  75.6 us
    convert_element_type x1, other arithmetic, whole_layer(): (own_part.astype(jnp.float32) + partner_part.astype(jnp.float32)).astype(...  2.12 us

commit v1 on v0

--- a/solution.py
+++ b/solution.py
@@ -242,15 +242,6 @@
 
 
 MESH = pl.DeviceIdType.MESH
-
-
-def flipped(index, mask, size):
-    total = 0
-    bit = 1
-    while bit < size:
-        total = total + lax.rem(lax.div(index, bit) + lax.div(mask, bit), 2) * bit
-        bit *= 2
-    return total
 
 
 def layer_kernel(
@@ -296,6 +287,7 @@
     relay_recv,
     kv_send,
     kv_recv,
+    forward_send,
     query_send,
     query_recv,
     contrast_send,
@@ -307,24 +299,37 @@
 ):
     f32 = jnp.float32
     bf16 = jnp.bfloat16
-    bands = sp_count // members
     sp = lax.axis_index("sp")
     tp = lax.axis_index("tp")
     other = 1 - tp
-    band = lax.div(sp, members)
+    plane = lax.div(sp, members)
     member = lax.rem(sp, members)
+    upper = lax.div(plane, 2)
+    side = lax.rem(plane, 2)
+    across = lax.div(member, 2)
+    along = lax.rem(member, 2)
+    half_count = 2 * members
     half, model = x_ref.shape
     rows = 2 * half
     width = gain.shape[1]
     head_dim = width // 2
-
+    chunks = 2
+    piece = half // chunks
+    in_lower = upper == 0
+    in_upper = upper == 1
+    crosses = plane == 1
+    relays = plane == 2
+    query_band = 2 * upper + tp
+    bands_of = (plane, plane + 1 - 2 * side, jnp.int32(1), jnp.int32(0))
+
+    half_columns = pl.ds(pl.multiple_of(side * 2 * width, 2 * width), 2 * width)
     loads = [
         pltpu.make_async_copy(src, dst, weight_sem.at[i])
         for i, (src, dst) in enumerate(
             (
-                (key_hbm, key_w),
-                (value_hbm, value_w),
-                (query_hbm, query_w),
+                (key_hbm.at[:, half_columns], key_w),
+                (value_hbm.at[:, half_columns], value_w),
+                (query_hbm.at[:, half_columns], query_w),
                 (pool_in_hbm, pool_in_w),
                 (pool_out_hbm, pool_out_w),
                 (contrast_hbm, contrast_w),
@@ -337,67 +342,171 @@
     keep.start()
 
     barrier = pltpu.get_barrier_semaphore()
-    greeted = [
-        (sp, other),
-        (lax.rem(sp + members, sp_count), tp),
-        (lax.rem(sp + sp_count - members, sp_count), tp),
-        (lax.rem(sp + 1, sp_count), tp),
-        (lax.rem(sp + sp_count - 1, sp_count), tp),
-    ]
-    greeted += [(band * members + flipped(member, j, members), tp) for j in range(1, members)]
-    for target in greeted:
+
+    def greet(target):
         pl.semaphore_signal(barrier, inc=1, device_id=target, device_id_type=MESH)
-    pl.semaphore_wait(barrier, len(greeted))
-
-    def pair_copy(step):
+
+    place = (side * members + member) * 2 + tp
+    for d in range(1, 2 * half_count):
+        goal = lax.rem(place + d, 2 * half_count)
+        greet((upper * half_count + lax.div(goal, 2), lax.rem(goal, 2)))
+
+    @pl.when(crosses)
+    def _():
+        greet((sp + members, tp))
+
+    @pl.when(relays)
+    def _():
+        greet((sp - members, tp))
+
+    @pl.when(sp == half_count - 1)
+    def _():
+        greet((sp + 1, tp))
+
+    @pl.when(sp == half_count)
+    def _():
+        greet((sp - 1, tp))
+
+    extra = jnp.where(jnp.logical_or(crosses, relays), 1, 0)
+    extra = extra + jnp.where(jnp.logical_or(sp == half_count - 1, sp == half_count), 1, 0)
+    pl.semaphore_wait(barrier, 2 * half_count - 1 + extra)
+
+    def cut(ch):
+        return pl.ds(ch * piece, piece)
+
+    pair_first = pltpu.make_async_remote_copy(
+        src_ref=x_ref,
+        dst_ref=rows_in.at[0, tp],
+        send_sem=pair_send.at[0, 0],
+        recv_sem=pair_recv.at[0, 0],
+        device_id=(sp, other),
+        device_id_type=MESH,
+    )
+
+    def pair_copy(step, ch):
         return pltpu.make_async_remote_copy(
-            src_ref=x_ref if step == 0 else rows_in.at[step, tp],
-            dst_ref=rows_in.at[step, tp],
-            send_sem=pair_send.at[step],
-            recv_sem=pair_recv.at[step],
+            src_ref=rows_in.at[step, tp, cut(ch)],
+            dst_ref=rows_in.at[step, tp, cut(ch)],
+            send_sem=pair_send.at[step, ch],
+            recv_sem=pair_recv.at[step, ch],
             device_id=(sp, other),
             device_id_type=MESH,
         )
 
-    def relay_copy(step):
+    def relay_copy(src, step, ch, target):
         return pltpu.make_async_remote_copy(
-            src_ref=x_ref if step == 1 else rows_in.at[step - 1, tp],
-            dst_ref=rows_in.at[step, tp],
-            send_sem=relay_send.at[step],
-            recv_sem=relay_recv.at[step],
-            device_id=(lax.rem(sp + members, sp_count), tp),
+            src_ref=src.at[cut(ch)],
+            dst_ref=rows_in.at[step, tp, cut(ch)],
+            send_sem=relay_send.at[step, ch],
+            recv_sem=relay_recv.at[step, ch],
+            device_id=(target, tp),
             device_id_type=MESH,
         )
 
+    def swap(ch):
+        return relay_copy(x_ref, 1, ch, sp + members * (1 - 2 * side))
+
+    def own_up(ch):
+        return relay_copy(x_ref, 2, ch, sp + members)
+
+    def low_up(ch):
+        return relay_copy(rows_in.at[1, tp], 3, ch, sp + members)
+
+    def pass_up(step, ch):
+        return relay_copy(rows_in.at[step, tp], step, ch, sp + members)
+
+    def top(step):
+        if step == 0:
+            return side == 1
+        if step == 1:
+            return side == 0
+        return jnp.bool_(False)
+
     def kv_copy(step, j):
+        goal = 2 * tp + j
+        first = jnp.where(top(step), 1, along)
         return pltpu.make_async_remote_copy(
             src_ref=kv_stage.at[step, j],
             dst_ref=kv.at[step, member],
             send_sem=kv_send.at[step, j],
-            recv_sem=kv_recv.at[step, j],
-            device_id=(band * members + flipped(member, j, members), tp),
+            recv_sem=kv_recv.at[step, member],
+            device_id=(plane * members + goal, first),
             device_id_type=MESH,
         )
 
-    def query_copy(j):
+    def forward_copy(step, source):
         return pltpu.make_async_remote_copy(
-            src_ref=query_stage.at[j],
+            src_ref=kv.at[step, source],
+            dst_ref=kv.at[step, source],
+            send_sem=forward_send.at[step, source],
+            recv_sem=kv_recv.at[step, source],
+            device_id=(sp, other),
+            device_id_type=MESH,
+        )
+
+    def query_copy(step, j):
+        core = jnp.where(top(step), 1, 0)
+        return pltpu.make_async_remote_copy(
+            src_ref=query_stage.at[step, j],
             dst_ref=queries.at[member],
-            send_sem=query_send.at[j],
-            recv_sem=query_recv.at[j],
-            device_id=(band * members + flipped(member, j, members), tp),
+            send_sem=query_send.at[step, j],
+            recv_sem=query_recv.at[member],
+            device_id=(plane * members + 2 * tp + j, core),
             device_id_type=MESH,
         )
 
-    def contrast_copy(j):
+    own_goal = across == tp
+
+    def own_stays(step, j):
+        return jnp.logical_and(own_goal, j == along)
+
+    def query_stays(step, j):
+        return jnp.logical_and(own_stays(step, j), jnp.where(top(step), 1, 0) == tp)
+
+    def own_forwards(step):
+        return jnp.logical_and(
+            own_goal, jnp.logical_or(jnp.logical_not(top(step)), tp == 0)
+        )
+
+    def passes_on(step, source):
+        mine = jnp.logical_and(source % 2 == tp, jnp.logical_not(top(step)))
+        return jnp.logical_and(source != member, mine)
+
+    def awaits(step, source):
+        needed = jnp.logical_or(tp == 1, jnp.logical_not(top(step)))
+        made_here = jnp.logical_and(source == member, own_goal)
+        return jnp.logical_and(needed, jnp.logical_not(made_here))
+
+    def contrast_stays(i):
+        return jnp.logical_and(
+            jnp.logical_and(query_band == plane, i == member), across == tp
+        )
+
+    head_here = 2 * side + along
+
+    def contrast_copy(i):
         return pltpu.make_async_remote_copy(
-            src_ref=contrast_stage.at[j],
-            dst_ref=contrasts.at[member],
-            send_sem=contrast_send.at[j],
-            recv_sem=contrast_recv.at[j],
-            device_id=(band * members + flipped(member, j, members), tp),
+            src_ref=contrast_stage.at[i],
+            dst_ref=contrasts.at[head_here],
+            send_sem=contrast_send.at[i],
+            recv_sem=contrast_recv.at[head_here],
+            device_id=(query_band * members + i, across),
             device_id_type=MESH,
         )
+
+    def contrast_incoming(head):
+        return pltpu.make_async_remote_copy(
+            src_ref=contrast_stage.at[0],
+            dst_ref=contrasts.at[head],
+            send_sem=contrast_send.at[0],
+            recv_sem=contrast_recv.at[head],
+            device_id=(sp, other),
+            device_id_type=MESH,
+        )
+
+    def contrast_local(head):
+        same = jnp.logical_and(head // 2 == side, 2 * tp + head % 2 == member)
+        return jnp.logical_and(same, side == tp)
 
     rim_copy = pltpu.make_async_remote_copy(
         src_ref=rim_stage,
@@ -416,151 +525,169 @@
         device_id_type=MESH,
     )
 
-    pair_copy(0).start()
-
-    @pl.when(band + 1 < bands)
-    def _():
-        relay_copy(1).start()
+    pair_first.start()
+    for ch in range(chunks):
+        swap(ch).start()
+
+        @pl.when(crosses)
+        def _(ch=ch):
+            own_up(ch).start()
+
+    peaks[...] = jnp.full(peaks.shape, -1e30, f32)
+    totals[...] = jnp.zeros(totals.shape, f32)
+    weighted[...] = jnp.zeros(weighted.shape, f32)
 
     def project(step):
         def one(t, carry):
-            j = lax.rem(t + 1, members)
-            head = flipped(member, j, members)
-            columns = pl.ds(pl.multiple_of(head * width, width), width)
+            j = jnp.where(t == 0, 1 - along, along)
+            columns = pl.ds(pl.multiple_of(j * width, width), width)
             x = rows_in[step].reshape(rows, model)
             keys = jnp.dot(x, key_w[:, columns], preferred_element_type=f32).astype(bf16)
             values = jnp.dot(x, value_w[:, columns], preferred_element_type=f32).astype(bf16)
-
-            @pl.when(j > 0)
+            stays = own_stays(step, j)
+
+            @pl.when(jnp.logical_not(stays))
             def _():
                 kv_stage[step, j, :, :width] = keys
                 kv_stage[step, j, :, width:] = values
                 kv_copy(step, j).start()
 
-            @pl.when(j == 0)
+            @pl.when(stays)
             def _():
                 kv[step, member, :, :width] = keys
                 kv[step, member, :, width:] = values
 
-            if step == 0:
+                @pl.when(own_forwards(step))
+                def _():
+                    forward_copy(step, member).start()
+
+            if step < 2:
                 mine = jnp.dot(x, query_w[:, columns], preferred_element_type=f32).astype(bf16)
-
-                @pl.when(j > 0)
+                kept = query_stays(step, j)
+
+                @pl.when(jnp.logical_not(kept))
                 def _():
-                    query_stage[j] = mine
-                    query_copy(j).start()
-
-                @pl.when(j == 0)
+                    query_stage[step, j] = mine
+                    query_copy(step, j).start()
+
+                @pl.when(kept)
                 def _():
                     queries[member] = mine
 
             return carry
 
-        lax.fori_loop(0, members, one, 0)
-
-    def take_band(step):
-        @pl.when(band >= step)
+        lax.fori_loop(0, 2, one, 0)
+
+    def take_swap(ch):
+        swap(ch).wait_recv()
+
+        @pl.when(crosses)
         def _():
-            relay_copy(step).wait_recv()
-            if step + 1 < bands:
-
-                @pl.when(band + 1 < bands)
-                def _():
-                    relay_copy(step + 1).start()
-
-            pair_copy(step).start()
-            pair_copy(step).wait_recv()
-            project(step)
+            low_up(ch).start()
+
+        pair_copy(1, ch).start()
+
+    def take_far(step, ch):
+        pass_up(step, ch).wait_recv()
+
+        @pl.when(relays)
+        def _():
+            pass_up(step, ch).start()
+
+        pair_copy(step, ch).start()
+
+    def paired(step):
+        for ch in range(chunks):
+            pair_copy(step, ch).wait_recv()
 
     log_scale = head_dim ** (-0.5) * math.log2(math.e)
 
-    def attend_block(step, i, blocks):
-        seen = len(blocks)
+    def attend_block(step, i, seen, masked):
         for u in range(2):
             cols = slice(u * head_dim, (u + 1) * head_dim)
-            keys = jnp.concatenate([kv[step, b, :, cols] for b in blocks], axis=0)
-            values = jnp.concatenate([kv[step, b, :, width:] for b in blocks], axis=0)
+            keys = kv[step, :seen, :, cols].reshape(seen * rows, head_dim)
+            values = kv[step, :seen, :, width:].reshape(seen * rows, width)
             scores = lax.dot_general(
                 queries[i, :, cols], keys, (((1,), (1,)), ((), ())), preferred_element_type=f32
             )
-            if step == 0:
+            if masked:
                 query_order = lax.broadcasted_iota(jnp.int32, scores.shape, 0) + (seen - 1) * rows
                 key_order = lax.broadcasted_iota(jnp.int32, scores.shape, 1)
                 scores = jnp.where(key_order <= query_order, scores, -jnp.inf)
-            peak = jnp.max(scores, axis=1, keepdims=True)
-            if step > 0:
-                old = peaks[u, i][:, :1]
-                peak = jnp.maximum(peak, old)
-                shrink = jnp.exp2((old - peak) * log_scale)
+            old = peaks[u, i][:, :1]
+            peak = jnp.maximum(jnp.max(scores, axis=1, keepdims=True), old)
+            shrink = jnp.exp2((old - peak) * log_scale)
             raised = jnp.exp2((scores - peak) * log_scale)
             total = jnp.sum(raised, axis=1, keepdims=True)
             update = jnp.dot(raised.astype(bf16), values, preferred_element_type=f32)
-            if step > 0:
-                total = total + totals[u, i][:, :1] * shrink
-                update = update + weighted[u, i] * shrink
+            total = total + totals[u, i][:, :1] * shrink
+            update = update + weighted[u, i] * shrink
             peaks[u, i] = jnp.broadcast_to(peak, peaks.shape[2:])
             totals[u, i] = jnp.broadcast_to(total, totals.shape[2:])
             weighted[u, i] = update
 
-    weight = balance[tp * members + member]
-
-    def finish(i, j):
+    weight = balance[across * members + head_here]
+
+    def finish(i):
         first = (weighted[0, i] / totals[0, i][:, :1]).astype(bf16).astype(f32)
         second = (weighted[1, i] / totals[1, i][:, :1]).astype(bf16).astype(f32)
         contrast = first - weight * second
         mean_square = jnp.mean(contrast * contrast, axis=1, keepdims=True)
         result = (contrast * lax.rsqrt(mean_square + norm_epsilon) * gain[...]).astype(bf16)
-
-        @pl.when(j > 0)
+        stays = contrast_stays(i)
+
+        @pl.when(jnp.logical_not(stays))
         def _():
-            contrast_stage[j] = result
-            contrast_copy(j).start()
-
-        @pl.when(j == 0)
+            contrast_stage[i] = result
+            contrast_copy(i).start()
+
+        @pl.when(stays)
         def _():
-            contrasts[member] = result
-
-    def attend_own():
-        for j in range(1, members):
-            query_copy(j).wait_recv()
-            kv_copy(0, j).wait_recv()
-        for i in range(members):
-            attend_block(0, i, list(range(i + 1)))
-
-            @pl.when(band == 0)
-            def _(i=i):
-                finish(i, flipped(member, i, members))
-
-    parts = (list(range(members)),)
-
-    def attend_band(step):
-        @pl.when(band >= step)
+            contrasts[head_here] = result
+
+    def each_block(work):
+        def one(t, carry):
+            work(lax.rem(member + 1 + t, members))
+            return carry
+
+        lax.fori_loop(0, members, one, 0)
+
+    def arrive(step):
+        for source in range(members):
+
+            @pl.when(awaits(step, source))
+            def _(source=source):
+                forward_copy(step, source).wait_recv()
+
+            @pl.when(passes_on(step, source))
+            def _(source=source):
+                forward_copy(step, source).start()
+
+    def attend(step):
+        band = bands_of[step]
+        arrive(step)
+
+        if step < 2:
+
+            @pl.when(band == query_band)
+            def _():
+                for i in range(members):
+                    attend_block(step, i, i + 1, True)
+
+        @pl.when(band < query_band)
         def _():
-            for part in parts:
-                for j in part:
-                    if j > 0:
-                        kv_copy(step, j).wait_recv()
-                blocks = [flipped(member, j, members) for j in part]
-
-                def one(t, carry, part=part, blocks=blocks):
-                    j = lax.rem(t + 1, members)
-                    i = flipped(member, j, members)
-                    attend_block(step, i, blocks)
-                    if part is parts[-1]:
-
-                        @pl.when(band == step)
-                        def _():
-                            finish(i, j)
-
-                    return carry
-
-                lax.fori_loop(0, members, one, 0)
+            def work(i):
+                attend_block(step, i, members, False)
+                if step == 3:
+                    finish(i)
+
+            each_block(work)
 
     keep.wait()
     loads[0].wait()
     loads[1].wait()
     loads[2].wait()
-    pair_copy(0).wait_recv()
+    pair_first.wait_recv()
     project(0)
 
     loads[3].wait()
@@ -573,7 +700,15 @@
     def _():
         rim_copy.start()
 
-    take_band(1)
+    for ch in range(chunks):
+        take_swap(ch)
+
+        @pl.when(relays)
+        def _(ch=ch):
+            take_far(2, ch)
+
+    paired(1)
+    project(1)
 
     @pl.when(sp > 0)
     def _():
@@ -609,80 +744,163 @@
             pool_out, pool_out_w[:, start : start + chunk], preferred_element_type=f32
         )
 
-    for step in range(2, bands):
-        take_band(step)
-        if step == 2:
-            attend_own()
-        else:
-            attend_band(step - 2)
-    if bands == 2:
-        attend_own()
-    for step in range(max(bands - 2, 1), bands):
-        attend_band(step)
+    def query_incoming(source):
+        return pltpu.make_async_remote_copy(
+            src_ref=query_stage.at[0, 0],
+            dst_ref=queries.at[source],
+            send_sem=query_send.at[0, 0],
+            recv_sem=query_recv.at[source],
+            device_id=(sp, other),
+            device_id_type=MESH,
+        )
+
+    def take_queries():
+        for source in range(members):
+
+            @pl.when(jnp.logical_not(jnp.logical_and(source == member, own_goal)))
+            def _(source=source):
+                query_incoming(source).wait_recv()
+
+    take_queries()
+    attend(0)
+
+    @pl.when(in_upper)
+    def _():
+        @pl.when(jnp.logical_not(relays))
+        def _():
+            for ch in range(chunks):
+                take_far(2, ch)
+
+        paired(2)
+        project(2)
+
+        @pl.when(relays)
+        def _():
+            for ch in range(chunks):
+                take_far(3, ch)
+
+    attend(1)
+
+    @pl.when(in_lower)
+    def _():
+        each_block(finish)
+
+    @pl.when(in_upper)
+    def _():
+        @pl.when(jnp.logical_not(relays))
+        def _():
+            for ch in range(chunks):
+                take_far(3, ch)
+
+        paired(3)
+        project(3)
+        attend(2)
+        attend(3)
 
     loads[5].wait()
-    for j in range(1, members):
-        contrast_copy(j).wait_recv()
-
-    def projected(side, store):
-        taken = pl.ds(pl.multiple_of(side * half, half), half)
+    for head in range(members):
+
+        @pl.when(jnp.logical_not(contrast_local(head)))
+        def _(head=head):
+            contrast_incoming(head).wait_recv()
+
+    def projected(taken_side, store):
+        taken = pl.ds(pl.multiple_of(taken_side * half, half), half)
         left = jnp.concatenate([contrasts[h, taken, :] for h in range(members)], axis=1)
         for start in range(0, model, chunk):
-            cut = slice(start, start + chunk)
-            part = jnp.dot(left, contrast_w[:, cut], preferred_element_type=f32)
-            store(cut, (part + pool_part[taken, cut]).astype(bf16))
-
-    def to_partner(cut, part):
-        out_stage[:, cut] = part
-
-    def to_self(cut, part):
-        out_ref[:, cut] = part
+            span = slice(start, start + chunk)
+            part = jnp.dot(left, contrast_w[:, span], preferred_element_type=f32)
+            store(span, (part + pool_part[taken, span]).astype(bf16))
+
+    def to_partner(span, part):
+        out_stage[:, span] = part
+
+    def to_self(span, part):
+        out_ref[:, span] = part
 
     projected(other, to_partner)
     out_copy.start()
     projected(tp, to_self)
     out_copy.wait()
-    pair_copy(0).wait_send()
-    for j in range(1, members):
-        query_copy(j).wait_send()
-        kv_copy(0, j).wait_send()
-        contrast_copy(j).wait_send()
+
+    pair_first.wait_send()
+    for ch in range(chunks):
+        swap(ch).wait_send()
+        pair_copy(1, ch).wait_send()
+
+        @pl.when(crosses)
+        def _(ch=ch):
+            own_up(ch).wait_send()
+            low_up(ch).wait_send()
+
+        @pl.when(relays)
+        def _(ch=ch):
+            pass_up(2, ch).wait_send()
+            pass_up(3, ch).wait_send()
+
+        @pl.when(in_upper)
+        def _(ch=ch):
+            pair_copy(2, ch).wait_send()
+            pair_copy(3, ch).wait_send()
+
+    def drain(step):
+        for j in range(2):
+
+            @pl.when(jnp.logical_not(own_stays(step, j)))
+            def _(j=j):
+                kv_copy(step, j).wait_send()
+
+            if step < 2:
+
+                @pl.when(jnp.logical_not(query_stays(step, j)))
+                def _(j=j):
+                    query_copy(step, j).wait_send()
+
+        @pl.when(own_forwards(step))
+        def _():
+            forward_copy(step, member).wait_send()
+
+        for source in range(members):
+
+            @pl.when(passes_on(step, source))
+            def _(source=source):
+                forward_copy(step, source).wait_send()
+
+    drain(0)
+    drain(1)
+
+    @pl.when(in_upper)
+    def _():
+        drain(2)
+        drain(3)
+
+    for i in range(members):
+
+        @pl.when(jnp.logical_not(contrast_stays(i)))
+        def _(i=i):
+            contrast_copy(i).wait_send()
 
     @pl.when(sp + 1 < sp_count)
     def _():
         rim_copy.wait_send()
 
-    for step in range(1, bands):
-
-        @pl.when(jnp.logical_and(band + 1 < bands, band >= step - 1))
-        def _(step=step):
-            relay_copy(step).wait_send()
-
-        @pl.when(band >= step)
-        def _(step=step):
-            pair_copy(step).wait_send()
-            for j in range(1, members):
-                kv_copy(step, j).wait_send()
-
-
-def kernel_scratch(sp_count, members, half, model, width, pool_cols):
+
+def kernel_scratch(members, half, model, width, pool_cols):
     bf16 = jnp.bfloat16
-    bands = sp_count // members
     rows = 2 * half
-    columns = members * width
     dma = pltpu.SemaphoreType.DMA
     return [
-        pltpu.VMEM((model, columns), bf16),
-        pltpu.VMEM((model, columns), bf16),
-        pltpu.VMEM((model, columns), bf16),
+        pltpu.VMEM((model, 2 * width), bf16),
+        pltpu.VMEM((model, 2 * width), bf16),
+        pltpu.VMEM((model, 2 * width), bf16),
         pltpu.VMEM((model, pool_cols), bf16),
-        pltpu.VMEM((columns, model), bf16),
+        pltpu.VMEM((members * width, model), bf16),
         pltpu.VMEM((pool_cols, model), bf16),
-        pltpu.VMEM((bands, 2, half, model), bf16),
-        pltpu.VMEM((bands, members, rows, 2 * width), bf16),
-        pltpu.VMEM((bands, members, rows, 2 * width), bf16),
+        pltpu.VMEM((4, 2, half, model), bf16),
+        pltpu.VMEM((4, members, rows, 2 * width), bf16),
+        pltpu.VMEM((4, 2, rows, 2 * width), bf16),
         pltpu.VMEM((members, rows, width), bf16),
-        pltpu.VMEM((members, rows, width), bf16),
+        pltpu.VMEM((2, 2, rows, width), bf16),
         pltpu.VMEM((2, members, rows, 128), jnp.float32),
         pltpu.VMEM((2, members, rows, 128), jnp.float32),
         pltpu.VMEM((2, members, rows, width), jnp.float32),
@@ -694,13 +912,14 @@
         pltpu.VMEM((half, model), bf16),
         dma((6,)),
         dma,
-        dma((bands,)),
-        dma((bands,)),
-        dma((bands,)),
-        dma((bands,)),
-        dma((bands, members)),
-        dma((bands, members)),
-        dma((members,)),
+        dma((4, 2)),
+        dma((4, 2)),
+        dma((4, 2)),
+        dma((4, 2)),
+        dma((4, 2)),
+        dma((4, members)),
+        dma((4, members)),
+        dma((2, 2)),
         dma((members,)),
         dma((members,)),
         dma((members,)),
@@ -740,15 +959,11 @@
     half, model = normed.shape
     pool_cols = pool_in_weight.shape[1]
     groups_here = pool_weight.shape[0]
-    scratch = kernel_scratch(
-        sp_count, max(members, 1), half, model, width, pool_cols
-    )
+    scratch = kernel_scratch(max(members, 1), half, model, width, pool_cols)
     fits = (
         lax.axis_size("tp") == 2
-        and members > 1
-        and members & (members - 1) == 0
-        and sp_count % members == 0
-        and sp_count // members > 1
+        and members == 4
+        and sp_count == 4 * members
         and groups_here % 4 == 0
         and scratch_bytes(scratch) < vmem_most * 3 // 4
     )

time: 77.9 us -> 85.4 us (1.096)
  the two profiles are of different devices: /device:TPU:25 before, /device:TPU:17 now
where the time goes in v1:
time: 85.4 us; the launch traced here: 84.7 us
  Pallas kernels  82.6 us (97%)
  other arithmetic  2.12 us (2%)
    pallas_call x1, Pallas kernels, whole_layer(): pl.pallas_call(functools.partial(layer_kernel, sp_count, members), out_sh...  82.6 us
    convert_element_type x1, other arithmetic, whole_layer(): (own_part.astype(jnp.float32) + partner_part.astype(jnp.float32)).astype(...  2.12 us

profile of v1, /device:TPU:17, one launch (start us, length us, event | category | flops | bytes accessed | tf_op | source)
XLA Modules:
  0.0 84.7 jit_solution(11495220376499841781)
XLA Ops:
  0.0 82.6 %shard_map.100 = (bf16[128,2048]{1,0:T(8,128)(2,1)}, bf16[128,2048]{1,0:T(8,128)(2,1)}) custom-call(bf16[128,2048]{1,0:T(8,128)(2,1)} %x_ref.1, bf16[4,128,128]{2,1,0:T(8,128)(2,1)} %pool_weight.1, f32[8]{0:T(128)} %balance.1, f32[1,256]{1,0:T(1,128)} %bitcast.1, bf16[2048,1024]{1,0:T(8,128)(2,1)} %query_hbm.1, bf16[2048,1024]{1,0:T(8,128)(2,1)} %key_hbm.1, ...), custom_call_target="tpu_custom_call" | custom-call | tf_op jit(solution)/shard_map/pallas_call | solution.py:985
  82.6 2.1 %add_convert_fusion = bf16[128,2048]{1,0:T(8,128)(2,1)} fusion(bf16[128,2048]{1,0:T(8,128)(2,1)} %get-tuple-element.8, bf16[128,2048]{1,0:T(8,128)(2,1)} %get-tuple-element.7), kind=kLoop, calls=%fused_computation | loop fusion | flops 1048576 | bytes 1572864 | tf_op jit(solution)/shard_map/convert_element_type | solution.py:1006

commit v2 on v1

--- a/solution.py
+++ b/solution.py
@@ -268,6 +268,7 @@
     rows_in,
     kv,
     kv_stage,
+    far_stage,
     queries,
     query_stage,
     peaks,
@@ -288,6 +289,9 @@
     kv_send,
     kv_recv,
     forward_send,
+    far_send,
+    far_recv,
+    far_forward,
     query_send,
     query_recv,
     contrast_send,
@@ -320,16 +324,15 @@
     crosses = plane == 1
     relays = plane == 2
     query_band = 2 * upper + tp
-    bands_of = (plane, plane + 1 - 2 * side, jnp.int32(1), jnp.int32(0))
-
-    half_columns = pl.ds(pl.multiple_of(side * 2 * width, 2 * width), 2 * width)
+    bands_of = (plane, plane + 1 - 2 * side)
+
     loads = [
         pltpu.make_async_copy(src, dst, weight_sem.at[i])
         for i, (src, dst) in enumerate(
             (
-                (key_hbm.at[:, half_columns], key_w),
-                (value_hbm.at[:, half_columns], value_w),
-                (query_hbm.at[:, half_columns], query_w),
+                (key_hbm, key_w),
+                (value_hbm, value_w),
+                (query_hbm, query_w),
                 (pool_in_hbm, pool_in_w),
                 (pool_out_hbm, pool_out_w),
                 (contrast_hbm, contrast_w),
@@ -412,15 +415,8 @@
     def low_up(ch):
         return relay_copy(rows_in.at[1, tp], 3, ch, sp + members)
 
-    def pass_up(step, ch):
-        return relay_copy(rows_in.at[step, tp], step, ch, sp + members)
-
     def top(step):
-        if step == 0:
-            return side == 1
-        if step == 1:
-            return side == 0
-        return jnp.bool_(False)
+        return side == (1 if step == 0 else 0)
 
     def kv_copy(step, j):
         goal = 2 * tp + j
@@ -457,6 +453,43 @@
 
     own_goal = across == tp
 
+    def part(ch):
+        return pl.ds(ch * half, half)
+
+    def far_copy(step, ch, goal_side, j):
+        slot = goal_side * 2 + j
+        goal = (2 * upper + goal_side) * members + 2 * tp + j
+        return pltpu.make_async_remote_copy(
+            src_ref=far_stage.at[step - 2, slot, part(ch)],
+            dst_ref=kv.at[step, member, part(ch)],
+            send_sem=far_send.at[step - 2, slot, ch],
+            recv_sem=far_recv.at[step - 2, member, ch],
+            device_id=(goal, along),
+            device_id_type=MESH,
+        )
+
+    def far_pass(step, source, ch):
+        return pltpu.make_async_remote_copy(
+            src_ref=kv.at[step, source, part(ch)],
+            dst_ref=kv.at[step, source, part(ch)],
+            send_sem=far_forward.at[step - 2, source, ch],
+            recv_sem=far_recv.at[step - 2, source, ch],
+            device_id=(sp, other),
+            device_id_type=MESH,
+        )
+
+    def far_stays(goal_side, j):
+        return jnp.logical_and(goal_side == side, jnp.logical_and(own_goal, j == along))
+
+    def far_here(source):
+        return jnp.logical_and(relays, source == member)
+
+    def far_passes(source):
+        return jnp.logical_and(source % 2 == tp, jnp.logical_not(far_here(source)))
+
+    def far_awaits(source):
+        return jnp.logical_not(jnp.logical_and(far_here(source), own_goal))
+
     def own_stays(step, j):
         return jnp.logical_and(own_goal, j == along)
 
@@ -540,11 +573,22 @@
     def project(step):
         def one(t, carry):
             j = jnp.where(t == 0, 1 - along, along)
-            columns = pl.ds(pl.multiple_of(j * width, width), width)
+            columns = pl.ds(pl.multiple_of((2 * side + j) * width, width), width)
             x = rows_in[step].reshape(rows, model)
+            mine = jnp.dot(x, query_w[:, columns], preferred_element_type=f32).astype(bf16)
             keys = jnp.dot(x, key_w[:, columns], preferred_element_type=f32).astype(bf16)
             values = jnp.dot(x, value_w[:, columns], preferred_element_type=f32).astype(bf16)
+            kept = query_stays(step, j)
             stays = own_stays(step, j)
+
+            @pl.when(jnp.logical_not(kept))
+            def _():
+                query_stage[step, j] = mine
+                query_copy(step, j).start()
+
+            @pl.when(kept)
+            def _():
+                queries[member] = mine
 
             @pl.when(jnp.logical_not(stays))
             def _():
@@ -561,22 +605,37 @@
                 def _():
                     forward_copy(step, member).start()
 
-            if step < 2:
-                mine = jnp.dot(x, query_w[:, columns], preferred_element_type=f32).astype(bf16)
-                kept = query_stays(step, j)
-
-                @pl.when(jnp.logical_not(kept))
-                def _():
-                    query_stage[step, j] = mine
-                    query_copy(step, j).start()
-
-                @pl.when(kept)
-                def _():
-                    queries[member] = mine
-
             return carry
 
         lax.fori_loop(0, 2, one, 0)
+
+    def project_far(step, ch):
+        pair_copy(step, ch).wait_recv()
+
+        def one(t, carry):
+            goal_side = 1 - lax.div(t, 2)
+            j = jnp.where(lax.rem(t, 2) == 0, 1 - along, along)
+            columns = pl.ds(pl.multiple_of((2 * goal_side + j) * width, width), width)
+            x = rows_in[step, :, cut(ch), :].reshape(half, model)
+            keys = jnp.dot(x, key_w[:, columns], preferred_element_type=f32).astype(bf16)
+            values = jnp.dot(x, value_w[:, columns], preferred_element_type=f32).astype(bf16)
+            stays = far_stays(goal_side, j)
+
+            @pl.when(jnp.logical_not(stays))
+            def _():
+                far_stage[step - 2, goal_side * 2 + j, part(ch), :width] = keys
+                far_stage[step - 2, goal_side * 2 + j, part(ch), width:] = values
+                far_copy(step, ch, goal_side, j).start()
+
+            @pl.when(stays)
+            def _():
+                kv[step, member, part(ch), :width] = keys
+                kv[step, member, part(ch), width:] = values
+                far_pass(step, member, ch).start()
+
+            return carry
+
+        lax.fori_loop(0, 4, one, 0)
 
     def take_swap(ch):
         swap(ch).wait_recv()
@@ -588,12 +647,7 @@
         pair_copy(1, ch).start()
 
     def take_far(step, ch):
-        pass_up(step, ch).wait_recv()
-
-        @pl.when(relays)
-        def _():
-            pass_up(step, ch).start()
-
+        (own_up(ch) if step == 2 else low_up(ch)).wait_recv()
         pair_copy(step, ch).start()
 
     def paired(step):
@@ -602,11 +656,11 @@
 
     log_scale = head_dim ** (-0.5) * math.log2(math.e)
 
-    def attend_block(step, i, seen, masked):
+    def attend_block(step, i, seen, masked, span=slice(None)):
         for u in range(2):
             cols = slice(u * head_dim, (u + 1) * head_dim)
-            keys = kv[step, :seen, :, cols].reshape(seen * rows, head_dim)
-            values = kv[step, :seen, :, width:].reshape(seen * rows, width)
+            keys = kv[step, :seen, span, cols].reshape(-1, head_dim)
+            values = kv[step, :seen, span, width:].reshape(-1, width)
             scores = lax.dot_general(
                 queries[i, :, cols], keys, (((1,), (1,)), ((), ())), preferred_element_type=f32
             )
@@ -665,23 +719,26 @@
 
     def attend(step):
         band = bands_of[step]
-        arrive(step)
-
-        if step < 2:
-
-            @pl.when(band == query_band)
-            def _():
-                for i in range(members):
-                    attend_block(step, i, i + 1, True)
+
+        @pl.when(band == query_band)
+        def _():
+            for i in range(members):
+                attend_block(step, i, i + 1, True)
 
         @pl.when(band < query_band)
         def _():
-            def work(i):
-                attend_block(step, i, members, False)
-                if step == 3:
-                    finish(i)
-
-            each_block(work)
+            each_block(lambda i: attend_block(step, i, members, False))
+
+    def far_arrive(step, ch):
+        for source in range(members):
+
+            @pl.when(far_awaits(source))
+            def _(source=source):
+                far_pass(step, source, ch).wait_recv()
+
+            @pl.when(far_passes(source))
+            def _(source=source):
+                far_pass(step, source, ch).start()
 
     keep.wait()
     loads[0].wait()
@@ -700,15 +757,27 @@
     def _():
         rim_copy.start()
 
-    for ch in range(chunks):
-        take_swap(ch)
-
-        @pl.when(relays)
-        def _(ch=ch):
-            take_far(2, ch)
+    take_swap(0)
+
+    @pl.when(relays)
+    def _():
+        take_far(2, 0)
+        project_far(2, 0)
+
+    take_swap(1)
+
+    @pl.when(relays)
+    def _():
+        take_far(2, 1)
 
     paired(1)
     project(1)
+
+    @pl.when(relays)
+    def _():
+        project_far(2, 1)
+        take_far(3, 0)
+        project_far(3, 0)
 
     @pl.when(sp > 0)
     def _():
@@ -761,41 +830,36 @@
             def _(source=source):
                 query_incoming(source).wait_recv()
 
+    arrive(0)
     take_queries()
     attend(0)
 
+    @pl.when(relays)
+    def _():
+        take_far(3, 1)
+        project_far(3, 1)
+
+    arrive(1)
+    attend(1)
+
+    @pl.when(in_lower)
+    def _():
+        each_block(finish)
+
     @pl.when(in_upper)
     def _():
-        @pl.when(jnp.logical_not(relays))
-        def _():
-            for ch in range(chunks):
-                take_far(2, ch)
-
-        paired(2)
-        project(2)
-
-        @pl.when(relays)
-        def _():
-            for ch in range(chunks):
-                take_far(3, ch)
-
-    attend(1)
-
-    @pl.when(in_lower)
-    def _():
-        each_block(finish)
-
-    @pl.when(in_upper)
-    def _():
-        @pl.when(jnp.logical_not(relays))
-        def _():
-            for ch in range(chunks):
-                take_far(3, ch)
-
-        paired(3)
-        project(3)
-        attend(2)
-        attend(3)
+        far_arrive(2, 0)
+        far_arrive(2, 1)
+        each_block(lambda i: attend_block(2, i, members, False))
+        far_arrive(3, 0)
+        each_block(lambda i: attend_block(3, i, members, False, slice(0, half)))
+        far_arrive(3, 1)
+
+        def last(i):
+            attend_block(3, i, members, False, slice(half, rows))
+            finish(i)
+
+        each_block(last)
 
     loads[5].wait()
     for head in range(members):
@@ -835,13 +899,26 @@
 
         @pl.when(relays)
         def _(ch=ch):
-            pass_up(2, ch).wait_send()
-            pass_up(3, ch).wait_send()
+            for step in range(2, 4):
+                pair_copy(step, ch).wait_send()
+                for slot in range(4):
+
+                    @pl.when(jnp.logical_not(far_stays(slot // 2, slot % 2)))
+                    def _(step=step, slot=slot):
+                        far_copy(step, ch, slot // 2, slot % 2).wait_send()
+
+                @pl.when(own_goal)
+                def _(step=step):
+                    far_pass(step, member, ch).wait_send()
 
         @pl.when(in_upper)
         def _(ch=ch):
-            pair_copy(2, ch).wait_send()
-            pair_copy(3, ch).wait_send()
+            for step in range(2, 4):
+                for source in range(members):
+
+                    @pl.when(far_passes(source))
+                    def _(step=step, source=source):
+                        far_pass(step, source, ch).wait_send()
 
     def drain(step):
         for j in range(2):
@@ -850,11 +927,9 @@
             def _(j=j):
                 kv_copy(step, j).wait_send()
 
-            if step < 2:
-
-                @pl.when(jnp.logical_not(query_stays(step, j)))
-                def _(j=j):
-                    query_copy(step, j).wait_send()
+            @pl.when(jnp.logical_not(query_stays(step, j)))
+            def _(j=j):
+                query_copy(step, j).wait_send()
 
         @pl.when(own_forwards(step))
         def _():
@@ -868,11 +943,6 @@
 
     drain(0)
     drain(1)
-
-    @pl.when(in_upper)
-    def _():
-        drain(2)
-        drain(3)
 
     for i in range(members):
 
@@ -890,15 +960,16 @@
     rows = 2 * half
     dma = pltpu.SemaphoreType.DMA
     return [
-        pltpu.VMEM((model, 2 * width), bf16),
-        pltpu.VMEM((model, 2 * width), bf16),
-        pltpu.VMEM((model, 2 * width), bf16),
+        pltpu.VMEM((model, members * width), bf16),
+        pltpu.VMEM((model, members * width), bf16),
+        pltpu.VMEM((model, members * width), bf16),
         pltpu.VMEM((model, pool_cols), bf16),
         pltpu.VMEM((members * width, model), bf16),
         pltpu.VMEM((pool_cols, model), bf16),
         pltpu.VMEM((4, 2, half, model), bf16),
         pltpu.VMEM((4, members, rows, 2 * width), bf16),
-        pltpu.VMEM((4, 2, rows, 2 * width), bf16),
+        pltpu.VMEM((2, 2, rows, 2 * width), bf16),
+        pltpu.VMEM((2, 4, rows, 2 * width), bf16),
         pltpu.VMEM((members, rows, width), bf16),
         pltpu.VMEM((2, 2, rows, width), bf16),
         pltpu.VMEM((2, members, rows, 128), jnp.float32),
@@ -916,9 +987,12 @@
         dma((4, 2)),
         dma((4, 2)),
         dma((4, 2)),
-        dma((4, 2)),
-        dma((4, members)),
-        dma((4, members)),
+        dma((2, 2)),
+        dma((2, members)),
+        dma((2, members)),
+        dma((2, 4, 2)),
+        dma((2, members, 2)),
+        dma((2, members, 2)),
         dma((2, 2)),
         dma((members,)),
         dma((members,)),

time: 85.4 us -> 87 us (1.019)
  Pallas kernels: 82.6 us -> 84.8 us
    pallas_call x1, Pallas kernels: 82.6 us -> 84.8 us  [whole_layer(): pl.pallas_call(functools.partial(layer_kernel, sp_count, members), out_sh...]
where the time goes in v2:
time: 87 us; the launch traced here: 86.9 us
  Pallas kernels  84.8 us (97%)
  other arithmetic  2.12 us (2%)
    pallas_call x1, Pallas kernels, whole_layer(): pl.pallas_call(functools.partial(layer_kernel, sp_count, members), out_sh...  84.8 us
    convert_element_type x1, other arithmetic, whole_layer(): (own_part.astype(jnp.float32) + partner_part.astype(jnp.float32)).astype(...  2.12 us

profile of v2, /device:TPU:17, one launch (start us, length us, event | category | flops | bytes accessed | tf_op | source)
XLA Modules:
  0.0 86.9 jit_solution(5254233039700955328)
XLA Ops:
  0.0 84.8 %shard_map.100 = (bf16[128,2048]{1,0:T(8,128)(2,1)}, bf16[128,2048]{1,0:T(8,128)(2,1)}) custom-call(bf16[128,2048]{1,0:T(8,128)(2,1)} %x_ref.1, bf16[4,128,128]{2,1,0:T(8,128)(2,1)} %pool_weight.1, f32[8]{0:T(128)} %balance.1, f32[1,256]{1,0:T(1,128)} %bitcast.1, bf16[2048,1024]{1,0:T(8,128)(2,1)} %query_hbm.1, bf16[2048,1024]{1,0:T(8,128)(2,1)} %key_hbm.1, ...), custom_call_target="tpu_custom_call" | custom-call | tf_op jit(solution)/shard_map/pallas_call | solution.py:1059
  84.8 2.1 %add_convert_fusion = bf16[128,2048]{1,0:T(8,128)(2,1)} fusion(bf16[128,2048]{1,0:T(8,128)(2,1)} %get-tuple-element.8, bf16[128,2048]{1,0:T(8,128)(2,1)} %get-tuple-element.7), kind=kLoop, calls=%fused_computation | loop fusion | flops 1048576 | bytes 1572864 | tf_op jit(solution)/shard_map/convert_element_type | solution.py:1080

commit v3 on v2

--- a/solution.py
+++ b/solution.py
@@ -656,11 +656,11 @@
 
     log_scale = head_dim ** (-0.5) * math.log2(math.e)
 
-    def attend_block(step, i, seen, masked, span=slice(None)):
+    def attend_block(step, i, seen, masked):
         for u in range(2):
             cols = slice(u * head_dim, (u + 1) * head_dim)
-            keys = kv[step, :seen, span, cols].reshape(-1, head_dim)
-            values = kv[step, :seen, span, width:].reshape(-1, width)
+            keys = kv[step, :seen, :, cols].reshape(-1, head_dim)
+            values = kv[step, :seen, :, width:].reshape(-1, width)
             scores = lax.dot_general(
                 queries[i, :, cols], keys, (((1,), (1,)), ((), ())), preferred_element_type=f32
             )
@@ -706,16 +706,29 @@
 
         lax.fori_loop(0, members, one, 0)
 
-    def arrive(step):
+    def lands_here(step, source):
+        return jnp.logical_and(
+            source != member, jnp.where(top(step), 1, source % 2) == tp
+        )
+
+    def pass_on(step):
         for source in range(members):
 
-            @pl.when(awaits(step, source))
+            @pl.when(lands_here(step, source))
             def _(source=source):
                 forward_copy(step, source).wait_recv()
 
             @pl.when(passes_on(step, source))
             def _(source=source):
                 forward_copy(step, source).start()
+
+    def arrive(step):
+        for source in range(members):
+            passed = jnp.logical_not(lands_here(step, source))
+
+            @pl.when(jnp.logical_and(awaits(step, source), passed))
+            def _(source=source):
+                forward_copy(step, source).wait_recv()
 
     def attend(step):
         band = bands_of[step]
@@ -729,16 +742,21 @@
         def _():
             each_block(lambda i: attend_block(step, i, members, False))
 
+    def far_pass_on(step, ch):
+        for source in range(members):
+
+            @pl.when(far_passes(source))
+            def _(source=source):
+                far_pass(step, source, ch).wait_recv()
+                far_pass(step, source, ch).start()
+
     def far_arrive(step, ch):
         for source in range(members):
-
-            @pl.when(far_awaits(source))
+            passed = jnp.logical_not(far_passes(source))
+
+            @pl.when(jnp.logical_and(far_awaits(source), passed))
             def _(source=source):
                 far_pass(step, source, ch).wait_recv()
-
-            @pl.when(far_passes(source))
-            def _(source=source):
-                far_pass(step, source, ch).start()
 
     keep.wait()
     loads[0].wait()
@@ -830,8 +848,9 @@
             def _(source=source):
                 query_incoming(source).wait_recv()
 
+    pass_on(0)
+    take_queries()
     arrive(0)
-    take_queries()
     attend(0)
 
     @pl.when(relays)
@@ -839,24 +858,35 @@
         take_far(3, 1)
         project_far(3, 1)
 
-    arrive(1)
-    attend(1)
-
-    @pl.when(in_lower)
-    def _():
-        each_block(finish)
-
     @pl.when(in_upper)
     def _():
+        far_pass_on(2, 0)
+        far_pass_on(2, 1)
         far_arrive(2, 0)
         far_arrive(2, 1)
         each_block(lambda i: attend_block(2, i, members, False))
+
+    pass_on(1)
+
+    @pl.when(in_upper)
+    def _():
+        far_pass_on(3, 0)
+
+    arrive(1)
+    attend(1)
+
+    @pl.when(in_lower)
+    def _():
+        each_block(finish)
+
+    @pl.when(in_upper)
+    def _():
+        far_pass_on(3, 1)
         far_arrive(3, 0)
-        each_block(lambda i: attend_block(3, i, members, False, slice(0, half)))
         far_arrive(3, 1)
 
         def last(i):
-            attend_block(3, i, members, False, slice(half, rows))
+            attend_block(3, i, members, False)
             finish(i)
 
         each_block(last)

time: 87 us -> 64.7 us (0.74)
  Pallas kernels: 84.8 us -> 62.2 us
    pallas_call x1, Pallas kernels: 84.8 us -> 62.2 us  [whole_layer(): pl.pallas_call(functools.partial(layer_kernel, sp_count, members), out_sh...]
where the time goes in v3:
time: 64.7 us; the launch traced here: 64.3 us
  Pallas kernels  62.2 us (96%)
  other arithmetic  2.12 us (3%)
    pallas_call x1, Pallas kernels, whole_layer(): pl.pallas_call(functools.partial(layer_kernel, sp_count, members), out_sh...  62.2 us
    convert_element_type x1, other arithmetic, whole_layer(): (own_part.astype(jnp.float32) + partner_part.astype(jnp.float32)).astype(...  2.12 us

profile of v3, /device:TPU:17, one launch (start us, length us, event | category | flops | bytes accessed | tf_op | source)
XLA Modules:
  0.0 64.3 jit_solution(3844845025229220162)
XLA Ops:
  0.0 62.2 %shard_map.100 = (bf16[128,2048]{1,0:T(8,128)(2,1)}, bf16[128,2048]{1,0:T(8,128)(2,1)}) custom-call(bf16[128,2048]{1,0:T(8,128)(2,1)} %x_ref.1, bf16[4,128,128]{2,1,0:T(8,128)(2,1)} %pool_weight.1, f32[8]{0:T(128)} %balance.1, f32[1,256]{1,0:T(1,128)} %bitcast.1, bf16[2048,1024]{1,0:T(8,128)(2,1)} %query_hbm.1, bf16[2048,1024]{1,0:T(8,128)(2,1)} %key_hbm.1, ...), custom_call_target="tpu_custom_call" | custom-call | tf_op jit(solution)/shard_map/pallas_call | solution.py:1089
  62.2 2.1 %add_convert_fusion = bf16[128,2048]{1,0:T(8,128)(2,1)} fusion(bf16[128,2048]{1,0:T(8,128)(2,1)} %get-tuple-element.8, bf16[128,2048]{1,0:T(8,128)(2,1)} %get-tuple-element.7), kind=kLoop, calls=%fused_computation | loop fusion | flops 1048576 | bytes 1572864 | tf_op jit(solution)/shard_map/convert_element_type | solution.py:1110

commit v4 on v3

--- a/solution.py
+++ b/solution.py
@@ -317,6 +317,7 @@
     rows = 2 * half
     width = gain.shape[1]
     head_dim = width // 2
+    chunk = math.gcd(model, 512)
     chunks = 2
     piece = half // chunks
     in_lower = upper == 0
@@ -418,50 +419,47 @@
     def top(step):
         return side == (1 if step == 0 else 0)
 
-    def kv_copy(step, j):
+    def kv_copy(step, j, ch):
         goal = 2 * tp + j
         first = jnp.where(top(step), 1, along)
         return pltpu.make_async_remote_copy(
-            src_ref=kv_stage.at[step, j],
-            dst_ref=kv.at[step, member],
-            send_sem=kv_send.at[step, j],
-            recv_sem=kv_recv.at[step, member],
+            src_ref=kv_stage.at[step, j, :, cut(ch)],
+            dst_ref=kv.at[step, member, :, cut(ch)],
+            send_sem=kv_send.at[step, j, ch],
+            recv_sem=kv_recv.at[step, member, ch],
             device_id=(plane * members + goal, first),
             device_id_type=MESH,
         )
 
-    def forward_copy(step, source):
+    def forward_copy(step, source, ch):
         return pltpu.make_async_remote_copy(
-            src_ref=kv.at[step, source],
-            dst_ref=kv.at[step, source],
-            send_sem=forward_send.at[step, source],
-            recv_sem=kv_recv.at[step, source],
+            src_ref=kv.at[step, source, :, cut(ch)],
+            dst_ref=kv.at[step, source, :, cut(ch)],
+            send_sem=forward_send.at[step, source, ch],
+            recv_sem=kv_recv.at[step, source, ch],
             device_id=(sp, other),
             device_id_type=MESH,
         )
 
-    def query_copy(step, j):
+    def query_copy(step, j, ch):
         core = jnp.where(top(step), 1, 0)
         return pltpu.make_async_remote_copy(
-            src_ref=query_stage.at[step, j],
-            dst_ref=queries.at[member],
-            send_sem=query_send.at[step, j],
-            recv_sem=query_recv.at[member],
+            src_ref=query_stage.at[step, j, :, cut(ch)],
+            dst_ref=queries.at[member, :, cut(ch)],
+            send_sem=query_send.at[step, j, ch],
+            recv_sem=query_recv.at[member, ch],
             device_id=(plane * members + 2 * tp + j, core),
             device_id_type=MESH,
         )
 
     own_goal = across == tp
-
-    def part(ch):
-        return pl.ds(ch * half, half)
 
     def far_copy(step, ch, goal_side, j):
         slot = goal_side * 2 + j
         goal = (2 * upper + goal_side) * members + 2 * tp + j
         return pltpu.make_async_remote_copy(
-            src_ref=far_stage.at[step - 2, slot, part(ch)],
-            dst_ref=kv.at[step, member, part(ch)],
+            src_ref=far_stage.at[step - 2, slot, ch],
+            dst_ref=kv.at[step, member, ch],
             send_sem=far_send.at[step - 2, slot, ch],
             recv_sem=far_recv.at[step - 2, member, ch],
             device_id=(goal, along),
@@ -470,8 +468,8 @@
 
     def far_pass(step, source, ch):
         return pltpu.make_async_remote_copy(
-            src_ref=kv.at[step, source, part(ch)],
-            dst_ref=kv.at[step, source, part(ch)],
+            src_ref=kv.at[step, source, ch],
+            dst_ref=kv.at[step, source, ch],
             send_sem=far_forward.at[step - 2, source, ch],
             recv_sem=far_recv.at[step - 2, source, ch],
             device_id=(sp, other),
@@ -549,14 +547,18 @@
         device_id=(lax.rem(sp + 1, sp_count), tp),
         device_id_type=MESH,
     )
-    out_copy = pltpu.make_async_remote_copy(
-        src_ref=out_stage,
-        dst_ref=out_recv,
-        send_sem=out_send,
-        recv_sem=out_recv_sem,
-        device_id=(sp, other),
-        device_id_type=MESH,
-    )
+
+    def out_copy(start):
+        span = slice(start, start + chunk)
+        return pltpu.make_async_remote_copy(
+            src_ref=out_stage.at[:, span],
+            dst_ref=out_recv.at[:, span],
+            send_sem=out_send.at[start // chunk],
+            recv_sem=out_recv_sem.at[start // chunk],
+            device_id=(sp, other),
+            device_id_type=MESH,
+        )
+
 
     pair_first.start()
     for ch in range(chunks):
@@ -570,40 +572,50 @@
     totals[...] = jnp.zeros(totals.shape, f32)
     weighted[...] = jnp.zeros(weighted.shape, f32)
 
-    def project(step):
+    def project(step, pieces):
+        here = cut(pieces[0]) if len(pieces) == 1 else slice(None)
+
         def one(t, carry):
             j = jnp.where(t == 0, 1 - along, along)
             columns = pl.ds(pl.multiple_of((2 * side + j) * width, width), width)
-            x = rows_in[step].reshape(rows, model)
-            mine = jnp.dot(x, query_w[:, columns], preferred_element_type=f32).astype(bf16)
-            keys = jnp.dot(x, key_w[:, columns], preferred_element_type=f32).astype(bf16)
-            values = jnp.dot(x, value_w[:, columns], preferred_element_type=f32).astype(bf16)
+            x = rows_in[step, :, here, :].reshape(-1, model)
+
+            def through(held):
+                dot = jnp.dot(x, held[:, columns], preferred_element_type=f32)
+                return dot.astype(bf16).reshape(2, -1, width)
+
+            mine = through(query_w)
+            keys = through(key_w)
+            values = through(value_w)
             kept = query_stays(step, j)
             stays = own_stays(step, j)
 
             @pl.when(jnp.logical_not(kept))
             def _():
-                query_stage[step, j] = mine
-                query_copy(step, j).start()
+                query_stage[step, j, :, here] = mine
+                for ch in pieces:
+                    query_copy(step, j, ch).start()
 
             @pl.when(kept)
             def _():
-                queries[member] = mine
+                queries[member, :, here] = mine
 
             @pl.when(jnp.logical_not(stays))
             def _():
-                kv_stage[step, j, :, :width] = keys
-                kv_stage[step, j, :, width:] = values
-                kv_copy(step, j).start()
+                kv_stage[step, j, :, here, :width] = keys
+                kv_stage[step, j, :, here, width:] = values
+                for ch in pieces:
+                    kv_copy(step, j, ch).start()
 
             @pl.when(stays)
             def _():
-                kv[step, member, :, :width] = keys
-                kv[step, member, :, width:] = values
+                kv[step, member, :, here, :width] = keys
+                kv[step, member, :, here, width:] = values
 
                 @pl.when(own_forwards(step))
                 def _():
-                    forward_copy(step, member).start()
+                    for ch in pieces:
+                        forward_copy(step, member, ch).start()
 
             return carry
 
@@ -623,14 +635,14 @@
 
             @pl.when(jnp.logical_not(stays))
             def _():
-                far_stage[step - 2, goal_side * 2 + j, part(ch), :width] = keys
-                far_stage[step - 2, goal_side * 2 + j, part(ch), width:] = values
+                far_stage[step - 2, goal_side * 2 + j, ch, :, :width] = keys
+                far_stage[step - 2, goal_side * 2 + j, ch, :, width:] = values
                 far_copy(step, ch, goal_side, j).start()
 
             @pl.when(stays)
             def _():
-                kv[step, member, part(ch), :width] = keys
-                kv[step, member, part(ch), width:] = values
+                kv[step, member, ch, :, :width] = keys
+                kv[step, member, ch, :, width:] = values
                 far_pass(step, member, ch).start()
 
             return carry
@@ -650,19 +662,19 @@
         (own_up(ch) if step == 2 else low_up(ch)).wait_recv()
         pair_copy(step, ch).start()
 
-    def paired(step):
-        for ch in range(chunks):
-            pair_copy(step, ch).wait_recv()
+    def project_swap(ch):
+        pair_copy(1, ch).wait_recv()
+        project(1, (ch,))
 
     log_scale = head_dim ** (-0.5) * math.log2(math.e)
 
     def attend_block(step, i, seen, masked):
         for u in range(2):
             cols = slice(u * head_dim, (u + 1) * head_dim)
-            keys = kv[step, :seen, :, cols].reshape(-1, head_dim)
-            values = kv[step, :seen, :, width:].reshape(-1, width)
+            keys = kv[step, :seen, :, :, cols].reshape(-1, head_dim)
+            values = kv[step, :seen, :, :, width:].reshape(-1, width)
             scores = lax.dot_general(
-                queries[i, :, cols], keys, (((1,), (1,)), ((), ())), preferred_element_type=f32
+                queries[i, :, :, cols].reshape(rows, head_dim), keys, (((1,), (1,)), ((), ())), preferred_element_type=f32
             )
             if masked:
                 query_order = lax.broadcasted_iota(jnp.int32, scores.shape, 0) + (seen - 1) * rows
@@ -682,12 +694,14 @@
 
     weight = balance[across * members + head_here]
 
-    def finish(i):
+    def finished_block(i):
         first = (weighted[0, i] / totals[0, i][:, :1]).astype(bf16).astype(f32)
         second = (weighted[1, i] / totals[1, i][:, :1]).astype(bf16).astype(f32)
         contrast = first - weight * second
         mean_square = jnp.mean(contrast * contrast, axis=1, keepdims=True)
-        result = (contrast * lax.rsqrt(mean_square + norm_epsilon) * gain[...]).astype(bf16)
+        return (contrast * lax.rsqrt(mean_square + norm_epsilon) * gain[...]).astype(bf16)
+
+    def send_block(i, result):
         stays = contrast_stays(i)
 
         @pl.when(jnp.logical_not(stays))
@@ -699,12 +713,20 @@
         def _():
             contrasts[head_here] = result
 
-    def each_block(work):
+    def turn(t):
+        return lax.rem(member + 1 + t, members)
+
+    def block_pairs(work):
         def one(t, carry):
-            work(lax.rem(member + 1 + t, members))
+            work(turn(2 * t), turn(2 * t + 1))
             return carry
 
-        lax.fori_loop(0, members, one, 0)
+        lax.fori_loop(0, members // 2, one, 0)
+
+    def finish_pair(i, k):
+        results = finished_block(i), finished_block(k)
+        send_block(i, results[0])
+        send_block(k, results[1])
 
     def lands_here(step, source):
         return jnp.logical_and(
@@ -712,35 +734,56 @@
         )
 
     def pass_on(step):
-        for source in range(members):
-
-            @pl.when(lands_here(step, source))
-            def _(source=source):
-                forward_copy(step, source).wait_recv()
-
-            @pl.when(passes_on(step, source))
-            def _(source=source):
-                forward_copy(step, source).start()
+        for ch in range(chunks):
+            for source in range(members):
+
+                @pl.when(lands_here(step, source))
+                def _(source=source, ch=ch):
+                    forward_copy(step, source, ch).wait_recv()
+
+                @pl.when(passes_on(step, source))
+                def _(source=source, ch=ch):
+                    forward_copy(step, source, ch).start()
 
     def arrive(step):
-        for source in range(members):
-            passed = jnp.logical_not(lands_here(step, source))
-
-            @pl.when(jnp.logical_and(awaits(step, source), passed))
-            def _(source=source):
-                forward_copy(step, source).wait_recv()
+        for ch in range(chunks):
+            for source in range(members):
+                passed = jnp.logical_not(lands_here(step, source))
+
+                @pl.when(jnp.logical_and(awaits(step, source), passed))
+                def _(source=source, ch=ch):
+                    forward_copy(step, source, ch).wait_recv()
 
     def attend(step):
         band = bands_of[step]
+
+        def between():
+            if step == 0:
+
+                @pl.when(relays)
+                def _():
+                    take_far(3, 1)
 
         @pl.when(band == query_band)
         def _():
             for i in range(members):
+                if i == members // 2:
+                    between()
                 attend_block(step, i, i + 1, True)
 
         @pl.when(band < query_band)
         def _():
-            each_block(lambda i: attend_block(step, i, members, False))
+            def one(t, carry):
+                attend_block(step, turn(2 * t), members, False)
+                attend_block(step, turn(2 * t + 1), members, False)
+
+                @pl.when(t == 0)
+                def _():
+                    between()
+
+                return carry
+
+            lax.fori_loop(0, members // 2, one, 0)
 
     def far_pass_on(step, ch):
         for source in range(members):
@@ -763,7 +806,7 @@
     loads[1].wait()
     loads[2].wait()
     pair_first.wait_recv()
-    project(0)
+    project(0, tuple(range(chunks)))
 
     loads[3].wait()
     pool_input = jnp.dot(
@@ -780,6 +823,11 @@
     @pl.when(relays)
     def _():
         take_far(2, 0)
+
+    project_swap(0)
+
+    @pl.when(relays)
+    def _():
         project_far(2, 0)
 
     take_swap(1)
@@ -788,14 +836,92 @@
     def _():
         take_far(2, 1)
 
-    paired(1)
-    project(1)
+    project_swap(1)
 
     @pl.when(relays)
     def _():
         project_far(2, 1)
         take_far(3, 0)
+
+    pass_on(0)
+
+    @pl.when(relays)
+    def _():
         project_far(3, 0)
+
+    def query_incoming(source, ch):
+        return pltpu.make_async_remote_copy(
+            src_ref=query_stage.at[0, 0, :, cut(ch)],
+            dst_ref=queries.at[source, :, cut(ch)],
+            send_sem=query_send.at[0, 0, ch],
+            recv_sem=query_recv.at[source, ch],
+            device_id=(sp, other),
+            device_id_type=MESH,
+        )
+
+    def take_queries():
+        for source in range(members):
+
+            @pl.when(jnp.logical_not(jnp.logical_and(source == member, own_goal)))
+            def _(source=source):
+                for ch in range(chunks):
+                    query_incoming(source, ch).wait_recv()
+
+    idle_first = jnp.logical_and(in_upper, jnp.logical_and(side == 1, tp == 0))
+
+    @pl.when(idle_first)
+    def _():
+        far_pass_on(2, 0)
+        far_pass_on(2, 1)
+
+    take_queries()
+    arrive(0)
+    attend(0)
+
+    @pl.when(relays)
+    def _():
+        project_far(3, 1)
+
+    def far_pair(i, k):
+        attend_block(2, i, members, False)
+        attend_block(2, k, members, False)
+
+    @pl.when(in_upper)
+    def _():
+        @pl.when(jnp.logical_not(idle_first))
+        def _():
+            far_pass_on(2, 0)
+            far_pass_on(2, 1)
+
+        far_arrive(2, 0)
+        far_arrive(2, 1)
+        block_pairs(far_pair)
+
+    pass_on(1)
+
+    @pl.when(in_upper)
+    def _():
+        far_pass_on(3, 0)
+
+    arrive(1)
+    attend(1)
+
+    @pl.when(in_lower)
+    def _():
+        block_pairs(finish_pair)
+
+    @pl.when(in_upper)
+    def _():
+        far_pass_on(3, 1)
+        far_arrive(3, 0)
+        far_arrive(3, 1)
+
+        def last_pair(i, k):
+            attend_block(3, i, members, False)
+            attend_block(3, k, members, False)
+            finish_pair(i, k)
+
+        block_pairs(last_pair)
 
     @pl.when(sp > 0)
     def _():
@@ -825,71 +951,10 @@
             jnp.dot(spread, pool_weight[group], preferred_element_type=f32).astype(bf16)
         )
     pool_out = jnp.concatenate(mixed, axis=1)
-    chunk = math.gcd(model, 512)
     for start in range(0, model, chunk):
         pool_part[:, start : start + chunk] = jnp.dot(
             pool_out, pool_out_w[:, start : start + chunk], preferred_element_type=f32
         )
-
-    def query_incoming(source):
-        return pltpu.make_async_remote_copy(
-            src_ref=query_stage.at[0, 0],
-            dst_ref=queries.at[source],
-            send_sem=query_send.at[0, 0],
-            recv_sem=query_recv.at[source],
-            device_id=(sp, other),
-            device_id_type=MESH,
-        )
-
-    def take_queries():
-        for source in range(members):
-
-            @pl.when(jnp.logical_not(jnp.logical_and(source == member, own_goal)))
-            def _(source=source):
-                query_incoming(source).wait_recv()
-
-    pass_on(0)
-    take_queries()
-    arrive(0)
-    attend(0)
-
-    @pl.when(relays)
-    def _():
-        take_far(3, 1)
-        project_far(3, 1)
-
-    @pl.when(in_upper)
-    def _():
-        far_pass_on(2, 0)
-        far_pass_on(2, 1)
-        far_arrive(2, 0)
-        far_arrive(2, 1)
-        each_block(lambda i: attend_block(2, i, members, False))
-
-    pass_on(1)
-
-    @pl.when(in_upper)
-    def _():
-        far_pass_on(3, 0)
-
-    arrive(1)
-    attend(1)
-
-    @pl.when(in_lower)
-    def _():
-        each_block(finish)
-
-    @pl.when(in_upper)
-    def _():
-        far_pass_on(3, 1)
-        far_arrive(3, 0)
-        far_arrive(3, 1)
-
-        def last(i):
-            attend_block(3, i, members, False)
-            finish(i)
-
-        each_block(last)
 
     loads[5].wait()
     for head in range(members):
@@ -908,14 +973,15 @@
 
     def to_partner(span, part):
         out_stage[:, span] = part
+        out_copy(span.start).start()
 
     def to_self(span, part):
         out_ref[:, span] = part
 
     projected(other, to_partner)
-    out_copy.start()
     projected(tp, to_self)
-    out_copy.wait()
+    for start in range(0, model, chunk):
+        out_copy(start).wait()
 
     pair_first.wait_send()
     for ch in range(chunks):
@@ -950,29 +1016,30 @@
                     def _(step=step, source=source):
                         far_pass(step, source, ch).wait_send()
 
-    def drain(step):
+    def drain(step, ch):
         for j in range(2):
 
             @pl.when(jnp.logical_not(own_stays(step, j)))
             def _(j=j):
-                kv_copy(step, j).wait_send()
+                kv_copy(step, j, ch).wait_send()
 
             @pl.when(jnp.logical_not(query_stays(step, j)))
             def _(j=j):
-                query_copy(step, j).wait_send()
+                query_copy(step, j, ch).wait_send()
 
         @pl.when(own_forwards(step))
         def _():
-            forward_copy(step, member).wait_send()
+            forward_copy(step, member, ch).wait_send()
 
         for source in range(members):
 
             @pl.when(passes_on(step, source))
             def _(source=source):
-                forward_copy(step, source).wait_send()
-
-    drain(0)
-    drain(1)
+                forward_copy(step, source, ch).wait_send()
+
+    for ch in range(chunks):
+        drain(0, ch)
+        drain(1, ch)
 
     for i in range(members):
 
@@ -997,11 +1064,11 @@
         pltpu.VMEM((members * width, model), bf16),
         pltpu.VMEM((pool_cols, model), bf16),
         pltpu.VMEM((4, 2, half, model), bf16),
-        pltpu.VMEM((4, members, rows, 2 * width), bf16),
-        pltpu.VMEM((2, 2, rows, 2 * width), bf16),
-        pltpu.VMEM((2, 4, rows, 2 * width), bf16),
-        pltpu.VMEM((members, rows, width), bf16),
-        pltpu.VMEM((2, 2, rows, width), bf16),
+        pltpu.VMEM((4, members, 2, half, 2 * width), bf16),
+        pltpu.VMEM((2, 2, 2, half, 2 * width), bf16),
+        pltpu.VMEM((2, 4, 2, half, 2 * width), bf16),
+        pltpu.VMEM((members, 2, half, width), bf16),
+        pltpu.VMEM((2, 2, 2, half, width), bf16),
         pltpu.VMEM((2, members, rows, 128), jnp.float32),
         pltpu.VMEM((2, members, rows, 128), jnp.float32),
         pltpu.VMEM((2, members, rows, width), jnp.float32),
@@ -1017,20 +1084,20 @@
         dma((4, 2)),
         dma((4, 2)),
         dma((4, 2)),
-        dma((2, 2)),
-        dma((2, members)),
-        dma((2, members)),
+        dma((2, 2, 2)),
+        dma((2, members, 2)),
+        dma((2, members, 2)),
         dma((2, 4, 2)),
         dma((2, members, 2)),
         dma((2, members, 2)),
-        dma((2, 2)),
-        dma((members,)),
+        dma((2, 2, 2)),
+        dma((members, 2)),
         dma((members,)),
         dma((members,)),
         dma,
         dma,
-        dma,
-        dma,
+        dma((model // math.gcd(model, 512),)),
+        dma((model // math.gcd(model, 512),)),
     ]
 
 

time: 64.7 us -> 64.6 us (level)
  no operation moved by 1% of the time
where the time goes in v4:
time: 64.6 us; the launch traced here: 64.4 us
  Pallas kernels  62.3 us (96%)
  other arithmetic  2.12 us (3%)
    pallas_call x1, Pallas kernels, whole_layer(): pl.pallas_call(functools.partial(layer_kernel, sp_count, members), out_sh...  62.3 us
    convert_element_type x1, other arithmetic, whole_layer(): (own_part.astype(jnp.float32) + partner_part.astype(jnp.float32)).astype(...  2.12 us

profile of v4, /device:TPU:17, one launch (start us, length us, event | category | flops | bytes accessed | tf_op | source)
XLA Modules:
  0.0 64.4 jit_solution(17906049751271150289)
XLA Ops:
  0.0 62.3 %shard_map.100 = (bf16[128,2048]{1,0:T(8,128)(2,1)}, bf16[128,2048]{1,0:T(8,128)(2,1)}) custom-call(bf16[128,2048]{1,0:T(8,128)(2,1)} %x_ref.1, bf16[4,128,128]{2,1,0:T(8,128)(2,1)} %pool_weight.1, f32[8]{0:T(128)} %balance.1, f32[1,256]{1,0:T(1,128)} %bitcast.1, bf16[2048,1024]{1,0:T(8,128)(2,1)} %query_hbm.1, bf16[2048,1024]{1,0:T(8,128)(2,1)} %key_hbm.1, ...), custom_call_target="tpu_custom_call" | custom-call | tf_op jit(solution)/shard_map/pallas_call | solution.py:1156
  62.3 2.1 %add_convert_fusion = bf16[128,2048]{1,0:T(8,128)(2,1)} fusion(bf16[128,2048]{1,0:T(8,128)(2,1)} %get-tuple-element.8, bf16[128,2048]{1,0:T(8,128)(2,1)} %get-tuple-element.7), kind=kLoop, calls=%fused_computation | loop fusion | flops 1048576 | bytes 1572864 | tf_op jit(solution)/shard_map/convert_element_type | solution.py:1177

commit v5 on v4

--- a/solution.py
+++ b/solution.py
@@ -247,10 +247,10 @@
 def layer_kernel(
     sp_count,
     members,
-    x_ref,
-    pool_weight,
-    balance,
-    gain,
+    x_hbm,
+    pool_weight_hbm,
+    balance_hbm,
+    gain_hbm,
     query_hbm,
     key_hbm,
     value_hbm,
@@ -259,6 +259,9 @@
     pool_out_hbm,
     out_ref,
     out_recv,
+    pool_weight,
+    balance,
+    gain,
     query_w,
     key_w,
     value_w,
@@ -313,7 +316,7 @@
     across = lax.div(member, 2)
     along = lax.rem(member, 2)
     half_count = 2 * members
-    half, model = x_ref.shape
+    half, model = x_hbm.shape
     rows = 2 * half
     width = gain.shape[1]
     head_dim = width // 2
@@ -327,23 +330,26 @@
     query_band = 2 * upper + tp
     bands_of = (plane, plane + 1 - 2 * side)
 
+    keep = pltpu.make_async_copy(x_hbm, rows_in.at[0, tp], local_sem)
+    keep.start()
+    x_ref = rows_in.at[0, tp]
+
     loads = [
         pltpu.make_async_copy(src, dst, weight_sem.at[i])
         for i, (src, dst) in enumerate(
             (
+                (query_hbm, query_w),
                 (key_hbm, key_w),
                 (value_hbm, value_w),
-                (query_hbm, query_w),
                 (pool_in_hbm, pool_in_w),
                 (pool_out_hbm, pool_out_w),
                 (contrast_hbm, contrast_w),
+                (pool_weight_hbm, pool_weight),
+                (balance_hbm, balance),
+                (gain_hbm, gain),
             )
         )
     ]
-    for load in loads:
-        load.start()
-    keep = pltpu.make_async_copy(x_ref, rows_in.at[0, tp], local_sem)
-    keep.start()
 
     barrier = pltpu.get_barrier_semaphore()
 
@@ -370,6 +376,9 @@
     @pl.when(sp == half_count)
     def _():
         greet((sp - 1, tp))
+
+    for load in loads:
+        load.start()
 
     extra = jnp.where(jnp.logical_or(crosses, relays), 1, 0)
     extra = extra + jnp.where(jnp.logical_or(sp == half_count - 1, sp == half_count), 1, 0)
@@ -560,6 +569,7 @@
         )
 
 
+    keep.wait()
     pair_first.start()
     for ch in range(chunks):
         swap(ch).start()
@@ -692,12 +702,10 @@
             totals[u, i] = jnp.broadcast_to(total, totals.shape[2:])
             weighted[u, i] = update
 
-    weight = balance[across * members + head_here]
-
     def finished_block(i):
-        first = (weighted[0, i] / totals[0, i][:, :1]).astype(bf16).astype(f32)
-        second = (weighted[1, i] / totals[1, i][:, :1]).astype(bf16).astype(f32)
-        contrast = first - weight * second
+        first = (weighted[0, i] * (1.0 / totals[0, i][:, :1])).astype(bf16).astype(f32)
+        second = (weighted[1, i] * (1.0 / totals[1, i][:, :1])).astype(bf16).astype(f32)
+        contrast = first - balance[across * members + head_here] * second
         mean_square = jnp.mean(contrast * contrast, axis=1, keepdims=True)
         return (contrast * lax.rsqrt(mean_square + norm_epsilon) * gain[...]).astype(bf16)
 
@@ -754,15 +762,8 @@
                 def _(source=source, ch=ch):
                     forward_copy(step, source, ch).wait_recv()
 
-    def attend(step):
+    def attend(step, between):
         band = bands_of[step]
-
-        def between():
-            if step == 0:
-
-                @pl.when(relays)
-                def _():
-                    take_far(3, 1)
 
         @pl.when(band == query_band)
         def _():
@@ -785,6 +786,10 @@
 
             lax.fori_loop(0, members // 2, one, 0)
 
+        @pl.when(band > query_band)
+        def _():
+            between()
+
     def far_pass_on(step, ch):
         for source in range(members):
 
@@ -801,7 +806,6 @@
             def _(source=source):
                 far_pass(step, source, ch).wait_recv()
 
-    keep.wait()
     loads[0].wait()
     loads[1].wait()
     loads[2].wait()
@@ -876,15 +880,32 @@
 
     take_queries()
     arrive(0)
-    attend(0)
+
+    def last_rows():
+        @pl.when(relays)
+        def _():
+            take_far(3, 1)
+
+    attend(0, last_rows)
 
     @pl.when(relays)
     def _():
         project_far(3, 1)
 
-    def far_pair(i, k):
-        attend_block(2, i, members, False)
-        attend_block(2, k, members, False)
+    def last_passes():
+        @pl.when(jnp.logical_and(in_upper, side == 1))
+        def _():
+            far_pass_on(3, 1)
+
+    def attend_swapped():
+        pass_on(1)
+
+        @pl.when(jnp.logical_and(in_upper, side == 1))
+        def _():
+            far_pass_on(3, 0)
+
+        arrive(1)
+        attend(1, last_passes)
 
     @pl.when(in_upper)
     def _():
@@ -893,26 +914,43 @@
             far_pass_on(2, 0)
             far_pass_on(2, 1)
 
+        @pl.when(relays)
+        def _():
+            attend_swapped()
+            far_pass_on(3, 0)
+
         far_arrive(2, 0)
         far_arrive(2, 1)
-        block_pairs(far_pair)
-
-    pass_on(1)
+
+        def one(t, carry):
+            attend_block(2, turn(2 * t), members, False)
+            attend_block(2, turn(2 * t + 1), members, False)
+
+            @pl.when(jnp.logical_and(t == 0, jnp.logical_and(relays, tp == 1)))
+            def _():
+                far_pass_on(3, 1)
+
+            return carry
+
+        lax.fori_loop(0, members // 2, one, 0)
+
+    @pl.when(jnp.logical_not(relays))
+    def _():
+        attend_swapped()
+
+    for load in loads[6:]:
+        load.wait()
+
+    @pl.when(in_lower)
+    def _():
+        block_pairs(finish_pair)
 
     @pl.when(in_upper)
     def _():
-        far_pass_on(3, 0)
-
-    arrive(1)
-    attend(1)
-
-    @pl.when(in_lower)
-    def _():
-        block_pairs(finish_pair)
-
-    @pl.when(in_upper)
-    def _():
-        far_pass_on(3, 1)
+        @pl.when(jnp.logical_and(relays, tp == 0))
+        def _():
+            far_pass_on(3, 1)
+
         far_arrive(3, 0)
         far_arrive(3, 1)
 
@@ -1052,11 +1090,15 @@
         rim_copy.wait_send()
 
 
-def kernel_scratch(members, half, model, width, pool_cols):
+def kernel_scratch(members, half, model, width, pool_cols, heads, groups_here):
     bf16 = jnp.bfloat16
     rows = 2 * half
+    group_width = pool_cols // groups_here
     dma = pltpu.SemaphoreType.DMA
     return [
+        pltpu.VMEM((groups_here, group_width, group_width), bf16),
+        pltpu.SMEM((heads,), jnp.float32),
+        pltpu.VMEM((1, width), jnp.float32),
         pltpu.VMEM((model, members * width), bf16),
         pltpu.VMEM((model, members * width), bf16),
         pltpu.VMEM((model, members * width), bf16),
@@ -1078,7 +1120,7 @@
         pltpu.VMEM((reach_back + 1, pool_cols), bf16),
         pltpu.VMEM((rows, model), jnp.float32),
         pltpu.VMEM((half, model), bf16),
-        dma((6,)),
+        dma((9,)),
         dma,
         dma((4, 2)),
         dma((4, 2)),
@@ -1102,6 +1144,7 @@
 
 
 vmem_most = 67043328
+kernel_grant = 54 * 2**20
 
 
 def scratch_bytes(scratch):
@@ -1130,7 +1173,10 @@
     half, model = normed.shape
     pool_cols = pool_in_weight.shape[1]
     groups_here = pool_weight.shape[0]
-    scratch = kernel_scratch(max(members, 1), half, model, width, pool_cols)
+    heads = map_balance.shape[0]
+    scratch = kernel_scratch(
+        max(members, 1), half, model, width, pool_cols, heads, groups_here
+    )
     fits = (
         lax.axis_size("tp") == 2
         and members == 4
@@ -1152,15 +1198,15 @@
             pool_out_weight,
         )
     vmem = pl.BlockSpec(memory_space=pltpu.VMEM)
-    hbm = pl.BlockSpec(memory_space=pl.ANY)
+    hbm = pl.BlockSpec(memory_space=pltpu.HBM)
     own_part, partner_part = pl.pallas_call(
         functools.partial(layer_kernel, sp_count, members),
-        out_shape=[jax.ShapeDtypeStruct((half, model), jnp.bfloat16)] * 2,
-        in_specs=[vmem, vmem, pl.BlockSpec(memory_space=pltpu.SMEM), vmem] + [hbm] * 6,
+        out_shape=[pltpu.VMEM((half, model), jnp.bfloat16)] * 2,
+        in_specs=[hbm] * 10,
         out_specs=[vmem, vmem],
         scratch_shapes=scratch,
         compiler_params=pltpu.CompilerParams(
-            collective_id=0, has_side_effects=True, vmem_limit_bytes=vmem_most
+            collective_id=0, has_side_effects=True, vmem_limit_bytes=kernel_grant
         ),
     )(
         normed,

time: 64.6 us -> 59.4 us (0.920)
  Pallas kernels: 62.3 us -> 58.3 us
  other arithmetic: 2.12 us -> 0.92 us
    pallas_call x1, Pallas kernels: 62.3 us -> 58.3 us  [whole_layer(): pl.pallas_call(functools.partial(layer_kernel, sp_count, members), out_sh...]
    convert_element_type x1, other arithmetic: 2.12 us -> 0.92 us  [whole_layer(): (own_part.astype(jnp.float32) + partner_part.astype(jnp.float32)).astype(...]
where the time goes in v5:
time: 59.4 us; the launch traced here: 59.2 us
  Pallas kernels  58.3 us (98%)
  other arithmetic  0.92 us (2%)
    pallas_call x1, Pallas kernels, whole_layer(): pl.pallas_call(functools.partial(layer_kernel, sp_count, members), out_sh...  58.3 us

profile of v5, /device:TPU:17, one launch (start us, length us, event | category | flops | bytes accessed | tf_op | source)
XLA Modules:
  0.0 59.2 jit_solution(6058708290852816756)
XLA Ops:
  0.0 58.3 %shard_map.100 = (bf16[128,2048]{1,0:T(8,128)(2,1)S(1)}, bf16[128,2048]{1,0:T(8,128)(2,1)S(1)}) custom-call(bf16[128,2048]{1,0:T(8,128)(2,1)} %x_hbm.1, bf16[4,128,128]{2,1,0:T(8,128)(2,1)} %pool_weight_hbm.1, f32[8]{0:T(128)} %balance_hbm.1, f32[1,256]{1,0:T(1,128)} %bitcast.1, bf16[2048,1024]{1,0:T(8,128)(2,1)} %query_hbm.1, bf16[2048,1024]{1,0:T(8,128)(2,1)} %key_hbm.1, ...), custom_call_target="tpu_custom_call" | custom-call | tf_op jit(solution)/shard_map/pallas_call | solution.py:1202
  58.3 0.9 %add_convert_fusion = bf16[128,2048]{1,0:T(8,128)(2,1)} fusion(bf16[128,2048]{1,0:T(8,128)(2,1)S(1)} %get-tuple-element.8, bf16[128,2048]{1,0:T(8,128)(2,1)S(1)} %get-tuple-element.7), kind=kLoop, calls=%fused_computation | loop fusion | flops 1048576 | bytes 1572864 | tf_op jit(solution)/shard_map/convert_element_type | solution.py:1223

commit v6 on v5

--- a/solution.py
+++ b/solution.py
@@ -334,13 +334,19 @@
     keep.start()
     x_ref = rows_in.at[0, tp]
 
+    near = pl.ds(pl.multiple_of(side * 2 * width, 2 * width), 2 * width)
+    far = pl.ds(pl.multiple_of((1 - side) * 2 * width, 2 * width), 2 * width)
+    far_loads = [
+        pltpu.make_async_copy(src.at[:, far], dst.at[:, far], weight_sem.at[9 + i])
+        for i, (src, dst) in enumerate(((key_hbm, key_w), (value_hbm, value_w)))
+    ]
     loads = [
         pltpu.make_async_copy(src, dst, weight_sem.at[i])
         for i, (src, dst) in enumerate(
             (
-                (query_hbm, query_w),
-                (key_hbm, key_w),
-                (value_hbm, value_w),
+                (query_hbm.at[:, near], query_w.at[:, near]),
+                (key_hbm.at[:, near], key_w.at[:, near]),
+                (value_hbm.at[:, near], value_w.at[:, near]),
                 (pool_in_hbm, pool_in_w),
                 (pool_out_hbm, pool_out_w),
                 (contrast_hbm, contrast_w),
@@ -377,7 +383,15 @@
     def _():
         greet((sp - 1, tp))
 
-    for load in loads:
+    for load in loads[:3]:
+        load.start()
+
+    @pl.when(relays)
+    def _():
+        for load in far_loads:
+            load.start()
+
+    for load in loads[3:]:
         load.start()
 
     extra = jnp.where(jnp.logical_or(crosses, relays), 1, 0)
@@ -832,6 +846,8 @@
 
     @pl.when(relays)
     def _():
+        for load in far_loads:
+            load.wait()
         project_far(2, 0)
 
     take_swap(1)
@@ -878,17 +894,22 @@
         far_pass_on(2, 0)
         far_pass_on(2, 1)
 
+    @pl.when(jnp.logical_and(relays, tp == 1))
+    def _():
+        take_far(3, 1)
+        project_far(3, 1)
+
     take_queries()
     arrive(0)
 
     def last_rows():
-        @pl.when(relays)
+        @pl.when(jnp.logical_and(relays, tp == 0))
         def _():
             take_far(3, 1)
 
     attend(0, last_rows)
 
-    @pl.when(relays)
+    @pl.when(jnp.logical_and(relays, tp == 0))
     def _():
         project_far(3, 1)
 
@@ -994,33 +1015,6 @@
             pool_out, pool_out_w[:, start : start + chunk], preferred_element_type=f32
         )
 
-    loads[5].wait()
-    for head in range(members):
-
-        @pl.when(jnp.logical_not(contrast_local(head)))
-        def _(head=head):
-            contrast_incoming(head).wait_recv()
-
-    def projected(taken_side, store):
-        taken = pl.ds(pl.multiple_of(taken_side * half, half), half)
-        left = jnp.concatenate([contrasts[h, taken, :] for h in range(members)], axis=1)
-        for start in range(0, model, chunk):
-            span = slice(start, start + chunk)
-            part = jnp.dot(left, contrast_w[:, span], preferred_element_type=f32)
-            store(span, (part + pool_part[taken, span]).astype(bf16))
-
-    def to_partner(span, part):
-        out_stage[:, span] = part
-        out_copy(span.start).start()
-
-    def to_self(span, part):
-        out_ref[:, span] = part
-
-    projected(other, to_partner)
-    projected(tp, to_self)
-    for start in range(0, model, chunk):
-        out_copy(start).wait()
-
     pair_first.wait_send()
     for ch in range(chunks):
         swap(ch).wait_send()
@@ -1079,15 +1073,35 @@
         drain(0, ch)
         drain(1, ch)
 
+    @pl.when(sp + 1 < sp_count)
+    def _():
+        rim_copy.wait_send()
+
+    loads[5].wait()
+    for head in range(members):
+
+        @pl.when(jnp.logical_not(contrast_local(head)))
+        def _(head=head):
+            contrast_incoming(head).wait_recv()
+
+    left = jnp.concatenate([contrasts[h] for h in range(members)], axis=1)
+    for start in range(0, model, chunk):
+        span = slice(start, start + chunk)
+        part = jnp.dot(left, contrast_w[:, span], preferred_element_type=f32)
+        part = part + pool_part[:, span]
+        low, high = part[:half], part[half:]
+        out_stage[:, span] = jnp.where(tp == 0, high, low).astype(bf16)
+        out_copy(start).start()
+        out_ref[:, span] = jnp.where(tp == 0, low, high).astype(bf16)
+
+    for start in range(0, model, chunk):
+        out_copy(start).wait()
+
     for i in range(members):
 
         @pl.when(jnp.logical_not(contrast_stays(i)))
         def _(i=i):
             contrast_copy(i).wait_send()
-
-    @pl.when(sp + 1 < sp_count)
-    def _():
-        rim_copy.wait_send()
 
 
 def kernel_scratch(members, half, model, width, pool_cols, heads, groups_here):
@@ -1120,7 +1134,7 @@
         pltpu.VMEM((reach_back + 1, pool_cols), bf16),
         pltpu.VMEM((rows, model), jnp.float32),
         pltpu.VMEM((half, model), bf16),
-        dma((9,)),
+        dma((11,)),
         dma,
         dma((4, 2)),
         dma((4, 2)),

time: 59.4 us -> 58.6 us (0.987)
  Pallas kernels: 58.3 us -> 57.5 us
    pallas_call x1, Pallas kernels: 58.3 us -> 57.5 us  [whole_layer(): pl.pallas_call(functools.partial(layer_kernel, sp_count, members), out_sh...]
where the time goes in v6:
time: 58.6 us; the launch traced here: 58.4 us
  Pallas kernels  57.5 us (98%)
  other arithmetic  0.92 us (2%)
    pallas_call x1, Pallas kernels, whole_layer(): pl.pallas_call(functools.partial(layer_kernel, sp_count, members), out_sh...  57.5 us

profile of v6, /device:TPU:17, one launch (start us, length us, event | category | flops | bytes accessed | tf_op | source)
XLA Modules:
  0.0 58.4 jit_solution(4280698461599197448)
XLA Ops:
  0.0 57.5 %shard_map.100 = (bf16[128,2048]{1,0:T(8,128)(2,1)S(1)}, bf16[128,2048]{1,0:T(8,128)(2,1)S(1)}) custom-call(bf16[128,2048]{1,0:T(8,128)(2,1)} %x_hbm.1, bf16[4,128,128]{2,1,0:T(8,128)(2,1)} %pool_weight_hbm.1, f32[8]{0:T(128)} %balance_hbm.1, f32[1,256]{1,0:T(1,128)} %bitcast.1, bf16[2048,1024]{1,0:T(8,128)(2,1)} %query_hbm.1, bf16[2048,1024]{1,0:T(8,128)(2,1)} %key_hbm.1, ...), custom_call_target="tpu_custom_call" | custom-call | tf_op jit(solution)/shard_map/pallas_call | solution.py:1216
  57.5 0.9 %add_convert_fusion = bf16[128,2048]{1,0:T(8,128)(2,1)} fusion(bf16[128,2048]{1,0:T(8,128)(2,1)S(1)} %get-tuple-element.8, bf16[128,2048]{1,0:T(8,128)(2,1)S(1)} %get-tuple-element.7), kind=kLoop, calls=%fused_computation | loop fusion | flops 1048576 | bytes 1572864 | tf_op jit(solution)/shard_map/convert_element_type | solution.py:1237

commit v7 on v6

--- a/solution.py
+++ b/solution.py
@@ -897,7 +897,6 @@
     @pl.when(jnp.logical_and(relays, tp == 1))
     def _():
         take_far(3, 1)
-        project_far(3, 1)
 
     take_queries()
     arrive(0)
@@ -907,6 +906,10 @@
         def _():
             take_far(3, 1)
 
+        @pl.when(jnp.logical_and(relays, tp == 1))
+        def _():
+            project_far(3, 1)
+
     attend(0, last_rows)
 
     @pl.when(jnp.logical_and(relays, tp == 0))
@@ -914,7 +917,7 @@
         project_far(3, 1)
 
     def last_passes():
-        @pl.when(jnp.logical_and(in_upper, side == 1))
+        @pl.when(jnp.logical_and(in_upper, jnp.logical_and(side == 1, tp == 1)))
         def _():
             far_pass_on(3, 1)
 
@@ -968,7 +971,7 @@
 
     @pl.when(in_upper)
     def _():
-        @pl.when(jnp.logical_and(relays, tp == 0))
+        @pl.when(tp == 0)
         def _():
             far_pass_on(3, 1)
 
@@ -1078,20 +1081,34 @@
         rim_copy.wait_send()
 
     loads[5].wait()
-    for head in range(members):
-
-        @pl.when(jnp.logical_not(contrast_local(head)))
-        def _(head=head):
-            contrast_incoming(head).wait_recv()
-
-    left = jnp.concatenate([contrasts[h] for h in range(members)], axis=1)
-    for start in range(0, model, chunk):
-        span = slice(start, start + chunk)
-        part = jnp.dot(left, contrast_w[:, span], preferred_element_type=f32)
-        part = part + pool_part[:, span]
+    def pair_of_heads(plane_side):
+        heads = (2 * plane_side, 2 * plane_side + 1)
+        for head in heads:
+
+            @pl.when(jnp.logical_not(contrast_local(head)))
+            def _(head=head):
+                contrast_incoming(head).wait_recv()
+
+        left = jnp.concatenate([contrasts[head] for head in heads], axis=1)
+        taken = pl.ds(pl.multiple_of(plane_side * 2 * width, 2 * width), 2 * width)
+
+        def product(span):
+            part = jnp.dot(left, contrast_w[taken, span], preferred_element_type=f32)
+            return part + pool_part[:, span]
+
+        return product
+
+    spans = [slice(start, start + chunk) for start in range(0, model, chunk)]
+    product = pair_of_heads(side)
+    for span in spans:
+        pool_part[:, span] = product(span)
+
+    product = pair_of_heads(1 - side)
+    for span in spans:
+        part = product(span)
         low, high = part[:half], part[half:]
         out_stage[:, span] = jnp.where(tp == 0, high, low).astype(bf16)
-        out_copy(start).start()
+        out_copy(span.start).start()
         out_ref[:, span] = jnp.where(tp == 0, low, high).astype(bf16)
 
     for start in range(0, model, chunk):

time: 58.6 us -> 57 us (0.973)
  Pallas kernels: 57.5 us -> 55.9 us
    pallas_call x1, Pallas kernels: 57.5 us -> 55.9 us  [whole_layer(): pl.pallas_call(functools.partial(layer_kernel, sp_count, members), out_sh...]
where the time goes in v7:
time: 57 us; the launch traced here: 56.8 us
  Pallas kernels  55.9 us (98%)
  other arithmetic  0.92 us (2%)
    pallas_call x1, Pallas kernels, whole_layer(): pl.pallas_call(functools.partial(layer_kernel, sp_count, members), out_sh...  55.9 us

profile of v7, /device:TPU:17, one launch (start us, length us, event | category | flops | bytes accessed | tf_op | source)
XLA Modules:
  0.0 56.8 jit_solution(3391859708694422292)
XLA Ops:
  0.0 55.9 %shard_map.100 = (bf16[128,2048]{1,0:T(8,128)(2,1)S(1)}, bf16[128,2048]{1,0:T(8,128)(2,1)S(1)}) custom-call(bf16[128,2048]{1,0:T(8,128)(2,1)} %x_hbm.1, bf16[4,128,128]{2,1,0:T(8,128)(2,1)} %pool_weight_hbm.1, f32[8]{0:T(128)} %balance_hbm.1, f32[1,256]{1,0:T(1,128)} %bitcast.1, bf16[2048,1024]{1,0:T(8,128)(2,1)} %query_hbm.1, bf16[2048,1024]{1,0:T(8,128)(2,1)} %key_hbm.1, ...), custom_call_target="tpu_custom_call" | custom-call | tf_op jit(solution)/shard_map/pallas_call | solution.py:1233
  55.9 0.9 %add_convert_fusion = bf16[128,2048]{1,0:T(8,128)(2,1)} fusion(bf16[128,2048]{1,0:T(8,128)(2,1)S(1)} %get-tuple-element.8, bf16[128,2048]{1,0:T(8,128)(2,1)S(1)} %get-tuple-element.7), kind=kLoop, calls=%fused_computation | loop fusion | flops 1048576 | bytes 1572864 | tf_op jit(solution)/shard_map/convert_element_type | solution.py:1254

commit v8 on v7

--- a/solution.py
+++ b/solution.py
@@ -921,15 +921,20 @@
         def _():
             far_pass_on(3, 1)
 
-    def attend_swapped():
-        pass_on(1)
+    def nothing():
+        pass
+
+    def attend_swapped(between):
+        @pl.when(jnp.logical_not(idle_first))
+        def _():
+            pass_on(1)
 
         @pl.when(jnp.logical_and(in_upper, side == 1))
         def _():
             far_pass_on(3, 0)
 
         arrive(1)
-        attend(1, last_passes)
+        attend(1, between)
 
     @pl.when(in_upper)
     def _():
@@ -940,7 +945,7 @@
 
         @pl.when(relays)
         def _():
-            attend_swapped()
+            attend_swapped(nothing)
             far_pass_on(3, 0)
 
         far_arrive(2, 0)
@@ -954,13 +959,17 @@
             def _():
                 far_pass_on(3, 1)
 
+            @pl.when(jnp.logical_and(t == 0, idle_first))
+            def _():
+                pass_on(1)
+
             return carry
 
         lax.fori_loop(0, members // 2, one, 0)
 
     @pl.when(jnp.logical_not(relays))
     def _():
-        attend_swapped()
+        attend_swapped(last_passes)
 
     for load in loads[6:]:
         load.wait()

time: 57 us -> 57.1 us (level)
  no operation moved by 1% of the time
where the time goes in v8:
time: 57.1 us; the launch traced here: 56.9 us
  Pallas kernels  55.9 us (98%)
  other arithmetic  0.92 us (2%)
    pallas_call x1, Pallas kernels, whole_layer(): pl.pallas_call(functools.partial(layer_kernel, sp_count, members), out_sh...  55.9 us

profile of v8, /device:TPU:17, one launch (start us, length us, event | category | flops | bytes accessed | tf_op | source)
XLA Modules:
  0.0 56.9 jit_solution(1486253539315745596)
XLA Ops:
  0.0 55.9 %shard_map.100 = (bf16[128,2048]{1,0:T(8,128)(2,1)S(1)}, bf16[128,2048]{1,0:T(8,128)(2,1)S(1)}) custom-call(bf16[128,2048]{1,0:T(8,128)(2,1)} %x_hbm.1, bf16[4,128,128]{2,1,0:T(8,128)(2,1)} %pool_weight_hbm.1, f32[8]{0:T(128)} %balance_hbm.1, f32[1,256]{1,0:T(1,128)} %bitcast.1, bf16[2048,1024]{1,0:T(8,128)(2,1)} %query_hbm.1, bf16[2048,1024]{1,0:T(8,128)(2,1)} %key_hbm.1, ...), custom_call_target="tpu_custom_call" | custom-call | tf_op jit(solution)/shard_map/pallas_call | solution.py:1242
  55.9 0.9 %add_convert_fusion = bf16[128,2048]{1,0:T(8,128)(2,1)} fusion(bf16[128,2048]{1,0:T(8,128)(2,1)S(1)} %get-tuple-element.8, bf16[128,2048]{1,0:T(8,128)(2,1)S(1)} %get-tuple-element.7), kind=kLoop, calls=%fused_computation | loop fusion | flops 1048576 | bytes 1572864 | tf_op jit(solution)/shard_map/convert_element_type | solution.py:1263
